TPU v7x, 32 devices: a whole 2x2x4 slice. The times are simulated.
32 devices in a mesh: sp: 8 (over z, core), tp: 4 (over y, x).
Axes of the slice: x: 2, y: 2, z: 4, core: 2. Of those that a mesh axis runs over, the one named last changes fastest.
Arguments:
- mix_values: bfloat16 [1024, 4096], P('sp', 'tp'), may hold values from -6 to 6
- mix_gate: bfloat16 [1024, 4096], P('sp', 'tp'), may hold values from -6 to 6
- input_keys: bfloat16 [1024, 2048], P('sp', 'tp'), may hold values from -0.31640625 to 0.31640625
- output_keys: bfloat16 [1024, 2048], P('sp', 'tp'), may hold values from -0.31640625 to 0.31640625
- step_sizes: float32 [1024, 64], P('sp', 'tp'), may hold values from 0.1 to 8
- decay_rates: float32 [64], P('tp'), may hold values from 4.8828125e-05 to 0.03
- out_proj: bfloat16 [2048, 4096], P('sp', 'tp'), may hold values from -0.09375 to 0.09375
- expert_inputs: bfloat16 [1024, 2048], P('sp'), may hold values from -20 to 20
- stream_grad: bfloat16 [1024, 2048], P('sp'), may hold values from -6 to 6
- routes: int32 [1024, 2], P('sp'), may hold values from 0 to 7, all different within a row; in each aligned block of 128 rows (0 to 127, 128 to 255, ...) at most 48 rows name the same one
- route_weights: float32 [1024, 2], P('sp'), may hold values from 0.1 to 0.9
- gate_proj: bfloat16 [8, 2048, 2048], P('sp', 'tp'), may hold values from -0.125 to 0.125
- up_proj: bfloat16 [8, 2048, 2048], P('sp', 'tp'), may hold values from -0.125 to 0.125
- down_proj: bfloat16 [8, 2048, 2048], P('sp', 'tp'), may hold values from -0.125 to 0.125
Outputs:
- grad_gate_proj: bfloat16 [8, 2048, 2048], P('sp', 'tp')
- grad_up_proj: bfloat16 [8, 2048, 2048], P('sp', 'tp')
- grad_down_proj: bfloat16 [8, 2048, 2048], P('sp', 'tp')
- grad_out_proj: float32 [2048, 4096], P('sp', 'tp')
- grad_values: bfloat16 [1024, 4096], P('sp', 'tp')
- grad_gate: bfloat16 [1024, 4096], P('sp', 'tp')
- grad_input_keys: bfloat16 [1024, 2048], P('sp', 'tp')
- grad_output_keys: bfloat16 [1024, 2048], P('sp', 'tp')
- grad_steps: float32 [1024, 64], P('sp', 'tp')
Inputs may be any that keep to these rules, and one draw needn't show every extreme that they name: In the rows of one device no expert is named by more than 48 routes, and on some devices one expert is named by exactly 48; the 2 routes of a token name different experts.
All inputs are finite; a program needn't handle non-finite values.
Results may differ from a plain program's by a relative error of at most 0.025.
Values may be sent and summed in bfloat16 or wider, within the bound.
A program may use at most 64 MiB of HBM per device.

v0:
```python
import jax
import jax.numpy as jnp
from jax import lax
from jax.sharding import PartitionSpec as P

NSTATE = 128
BLOCK = 128


CLAMP_LIMIT = 7.0
SIGMOID_SCALE = 1.702
HIGHEST = lax.Precision.HIGHEST


def prefix(x, axis, combine, identity, reverse):
    count, here = (lax.axis_size(axis), lax.axis_index(axis))
    everything = jax.tree.map(lambda part: lax.all_gather(part, axis), x)
    start = jax.tree.map(
        lambda part, zero: jnp.broadcast_to(jnp.asarray(zero, part.dtype), part.shape), x, identity
    )

    def lap(k, before):
        at = count - 1 - k if reverse else k
        reached = at > here if reverse else at < here
        new = combine(before, jax.tree.map(lambda part: part[at], everything))
        return jax.tree.map(lambda a, b: jnp.where(reached, a, b), new, before)

    return lax.fori_loop(0, count, lap, start)


def decay_span(head_values, in_keys, out_keys, head_steps, head_rates, start_state):
    length = head_values.shape[0]
    num_blocks = length // BLOCK
    causal_mask = jnp.tril(jnp.ones((BLOCK, BLOCK), dtype=bool))

    def advance(carry_state, block_data):
        block_values, block_in, block_out, block_steps = block_data
        log_decay = jnp.cumsum(-block_steps * head_rates, axis=0)
        weighted = block_values * block_steps[..., None]
        ordered = jnp.transpose(log_decay, (1, 2, 0))
        log_gaps = ordered[..., :, None] - ordered[..., None, :]
        mixing = jnp.where(causal_mask, jnp.exp(jnp.where(causal_mask, log_gaps, 0.0)), 0.0)
        scores = jnp.einsum("lgn,sgn->gls", block_out, block_in, precision=HIGHEST)
        within = jnp.einsum(
            "grls,sgrp->lgrp", scores[:, None] * mixing, weighted, precision=HIGHEST
        )
        carried = (
            jnp.einsum("lgn,grpn->lgrp", block_out, carry_state, precision=HIGHEST)
            * jnp.exp(log_decay)[..., None]
        )
        to_end = jnp.exp(log_decay[-1] - log_decay)
        new_state = carry_state * jnp.exp(log_decay[-1])[..., None, None] + jnp.einsum(
            "lgn,lgrp->grpn", block_in, weighted * to_end[..., None], precision=HIGHEST
        )
        return (new_state, within + carried)

    blocks = tuple(
        (
            whole_array.reshape((num_blocks, BLOCK) + whole_array.shape[1:])
            for whole_array in (head_values, in_keys, out_keys, head_steps)
        )
    )
    last_state, block_outputs = lax.scan(advance, start_state, blocks)
    return (block_outputs.reshape(head_values.shape), last_state)


def expert_backward(in_slots, grad_slots, gate_weight, up_weight, down_weight):
    model_width = in_slots.shape[-1]
    in_rows = in_slots.reshape(-1, model_width)
    grad_rows = grad_slots.reshape(-1, model_width)
    contract = (((1,), (1,)), ((), ()))
    across = (((0,), (0,)), ((), ()))
    gate_pre = lax.dot_general(in_rows, gate_weight, contract, preferred_element_type=jnp.float32)
    up_pre = lax.dot_general(in_rows, up_weight, contract, preferred_element_type=jnp.float32)
    gate_clamped = jnp.minimum(gate_pre, CLAMP_LIMIT)
    up_clamped = jnp.clip(up_pre, -CLAMP_LIMIT, CLAMP_LIMIT)
    gate_sigmoid = jax.nn.sigmoid(SIGMOID_SCALE * gate_clamped)
    activation = ((up_clamped + 1.0) * gate_clamped * gate_sigmoid).astype(jnp.bfloat16)
    act_grad = lax.dot_general(grad_rows, down_weight, contract, preferred_element_type=jnp.float32)
    gate_grad = jnp.where(
        gate_pre < CLAMP_LIMIT,
        act_grad
        * (up_clamped + 1.0)
        * gate_sigmoid
        * (1.0 + SIGMOID_SCALE * gate_clamped * (1.0 - gate_sigmoid)),
        0.0,
    ).astype(jnp.bfloat16)
    up_grad = jnp.where(
        jnp.abs(up_pre) < CLAMP_LIMIT, act_grad * gate_clamped * gate_sigmoid, 0.0
    ).astype(jnp.bfloat16)
    grad_down = lax.dot_general(
        activation, grad_rows, across, preferred_element_type=jnp.float32
    ).astype(jnp.bfloat16)
    grad_gate_w = lax.dot_general(
        gate_grad, in_rows, across, preferred_element_type=jnp.float32
    ).astype(jnp.bfloat16)
    grad_up_w = lax.dot_general(
        up_grad, in_rows, across, preferred_element_type=jnp.float32
    ).astype(jnp.bfloat16)
    input_grad = jnp.dot(gate_grad, gate_weight, preferred_element_type=jnp.float32) + jnp.dot(
        up_grad, up_weight, preferred_element_type=jnp.float32
    )
    return (grad_gate_w, grad_up_w, grad_down, input_grad.reshape(in_slots.shape))


def compose(earlier, later):
    return (earlier[0] * later[0], later[0][..., None, None] * earlier[1] + later[1])


def body(
    mix_values,
    mix_gate,
    input_keys,
    output_keys,
    step_sizes,
    decay_rates,
    out_proj,
    expert_inputs,
    stream_grad,
    routes,
    route_weights,
    gate_proj,
    up_proj,
    down_proj,
):
    tok_rows = mix_values.shape[0]
    model_width = stream_grad.shape[1]
    route_count = routes.shape[1]
    sp_devices = lax.axis_size("sp")
    tp_devices = lax.axis_size("tp")
    local_experts = gate_proj.shape[0]
    all_experts = local_experts * sp_devices
    capacity = 3 * tok_rows * route_count // (2 * all_experts)
    num_heads = step_sizes.shape[1]
    num_groups = input_keys.shape[1] // NSTATE
    per_group = num_heads // num_groups
    head_size = mix_values.shape[1] // num_heads
    across = (((0,), (0,)), ((), ()))
    flat_routes = routes.reshape(-1)
    one_hot = (flat_routes[:, None] == jnp.arange(all_experts, dtype=jnp.int32)[None, :]).astype(
        jnp.int32
    )
    slot_rank = jnp.sum((jnp.cumsum(one_hot, axis=0) - 1) * one_hot, axis=1)
    slot_index = flat_routes * capacity + slot_rank
    slot_table = (
        jnp.zeros((all_experts * capacity,), jnp.int32)
        .at[slot_index]
        .set(jnp.arange(tok_rows * route_count, dtype=jnp.int32) + 1)
    )
    slot_used = slot_table > 0
    route_id = jnp.maximum(slot_table - 1, 0)
    token_id = route_id // route_count
    route_scale = jnp.where(slot_used, route_weights.reshape(-1)[route_id], 0.0)
    send_grad = (
        (stream_grad[token_id].astype(jnp.float32) * route_scale[:, None])
        .astype(jnp.bfloat16)
        .reshape(all_experts, capacity, model_width)
    )
    send_rows = jnp.where(
        slot_used[:, None], expert_inputs[token_id], jnp.zeros((), jnp.bfloat16)
    ).reshape(all_experts, capacity, model_width)
    got_grad, got_rows = (
        lax.all_to_all(send_grad, "sp", split_axis=0, concat_axis=0, tiled=True),
        lax.all_to_all(send_rows, "sp", split_axis=0, concat_axis=0, tiled=True),
    )
    got_grad = got_grad.reshape(sp_devices, local_experts, capacity, model_width)
    got_rows = got_rows.reshape(sp_devices, local_experts, capacity, model_width)
    grad_gate_proj, grad_up_proj, grad_down_proj, partial_back = jax.vmap(
        expert_backward, in_axes=(1, 1, 0, 0, 0), out_axes=(0, 0, 0, 1)
    )(got_rows, got_grad, gate_proj, up_proj, down_proj)
    col_width = model_width // tp_devices
    column = lax.axis_index("tp")
    stream_cols = lax.dynamic_slice_in_dim(stream_grad, column * col_width, col_width, 1).astype(
        jnp.float32
    )
    reduced = lax.psum_scatter(
        partial_back.reshape(all_experts * capacity, model_width).astype(jnp.bfloat16),
        "tp",
        scatter_dimension=1,
        tiled=True,
    ).astype(jnp.float32)
    returned = lax.all_to_all(
        reduced.reshape(all_experts, capacity, col_width).astype(jnp.bfloat16),
        "sp",
        split_axis=0,
        concat_axis=0,
        tiled=True,
    ).astype(jnp.float32)
    summed = jnp.sum(
        returned.reshape(all_experts * capacity, col_width)[slot_index].reshape(
            tok_rows, route_count, col_width
        ),
        axis=1,
    )
    stream_part = (stream_cols + summed).astype(jnp.bfloat16)
    stream_total = lax.all_gather(stream_part, "tp", axis=1, tiled=True)
    head_values = mix_values.astype(jnp.float32).reshape(tok_rows, num_groups, per_group, head_size)
    in_keys = input_keys.astype(jnp.float32).reshape(tok_rows, num_groups, NSTATE)
    out_keys = output_keys.astype(jnp.float32).reshape(tok_rows, num_groups, NSTATE)
    head_steps = step_sizes.reshape(tok_rows, num_groups, per_group)
    head_rates = decay_rates.reshape(num_groups, per_group)
    zero_state = jnp.zeros((num_groups, per_group, head_size, NSTATE), jnp.float32)

    def local_span(values_in, keys_in, keys_out, steps_in):
        return decay_span(values_in, keys_in, keys_out, steps_in, head_rates, zero_state)

    (own_out, own_state), back_local = jax.vjp(
        local_span, head_values, in_keys, out_keys, head_steps
    )
    span_decay = jnp.exp(-jnp.sum(head_steps * head_rates, axis=0))
    identity = (jnp.ones_like(span_decay), jnp.zeros_like(own_state))
    state_in = prefix((span_decay, own_state), "sp", compose, identity, False)[1]

    def entering(state_value, keys_out, steps_in):
        decay_here = jnp.exp(jnp.cumsum(-steps_in * head_rates, axis=0))
        return (
            jnp.einsum("lgn,grpn->lgrp", keys_out, state_value, precision=HIGHEST)
            * decay_here[..., None]
        )

    enter_out, back_enter = jax.vjp(entering, state_in, out_keys, head_steps)
    mixer_out = own_out + enter_out
    gate_in = mix_gate.astype(jnp.float32).reshape(tok_rows, num_groups, per_group, head_size)
    gate_sigmoid = jax.nn.sigmoid(gate_in)
    gate_silu = gate_in * gate_sigmoid
    gated_out = (mixer_out * gate_silu).reshape(tok_rows, -1).astype(jnp.bfloat16)
    stream_part_cols = stream_total
    gated_grad = jnp.dot(
        stream_part_cols,
        lax.all_gather(out_proj, "sp", axis=0, tiled=True),
        preferred_element_type=jnp.float32,
    )
    gated_grad = gated_grad.reshape(tok_rows, num_groups, per_group, head_size)
    grad_gate = (
        (gated_grad * mixer_out * gate_sigmoid * (1.0 + gate_in * (1.0 - gate_sigmoid)))
        .reshape(tok_rows, -1)
        .astype(jnp.bfloat16)
    )
    mixer_grad = gated_grad * gate_silu
    state_grad, keys_grad_enter, steps_grad_enter = back_enter(mixer_grad)
    state_out_grad = prefix((span_decay, state_grad), "sp", compose, identity, True)[1]
    grad_vals, grad_in, keys_grad_own, steps_grad_own = back_local((mixer_grad, state_out_grad))
    decay_grad = -head_rates * span_decay * jnp.sum(state_out_grad * state_in, axis=(2, 3))
    grad_steps = (steps_grad_own + steps_grad_enter + decay_grad[None]).reshape(tok_rows, num_heads)
    stream_part_cols = stream_total
    grad_out_proj = lax.psum_scatter(
        lax.dot_general(
            stream_part_cols, gated_out, across, preferred_element_type=jnp.float32
        ).astype(jnp.bfloat16),
        "sp",
        scatter_dimension=0,
        tiled=True,
    ).astype(jnp.float32)
    return (
        grad_gate_proj,
        grad_up_proj,
        grad_down_proj,
        grad_out_proj,
        grad_vals.reshape(tok_rows, -1).astype(jnp.bfloat16),
        grad_gate,
        grad_in.reshape(tok_rows, -1).astype(jnp.bfloat16),
        (keys_grad_own + keys_grad_enter).reshape(tok_rows, -1).astype(jnp.bfloat16),
        grad_steps,
    )


def solution(mesh):
    return jax.shard_map(
        body,
        mesh=mesh,
        in_specs=(
            P("sp", "tp"),
            P("sp", "tp"),
            P("sp", "tp"),
            P("sp", "tp"),
            P("sp", "tp"),
            P("tp"),
            P("sp", "tp"),
            P("sp", None),
            P("sp", None),
            P("sp", None),
            P("sp", None),
            P("sp", "tp", None),
            P("sp", "tp", None),
            P("sp", "tp", None),
        ),
        out_specs=(
            P("sp", "tp", None),
            P("sp", "tp", None),
            P("sp", "tp", None),
            P("sp", "tp"),
            P("sp", "tp"),
            P("sp", "tp"),
            P("sp", "tp"),
            P("sp", "tp"),
            P("sp", "tp"),
        ),
        check_vma=False,
    )
```

profile of v0, /device:TPU:0, one launch (start us, length us, event | category | flops | bytes accessed | tf_op | source)
XLA Modules:
  0.0 339.8 jit_solution(10902424300172755170)
XLA Ops:
  22.3 6.5 %all-to-all-start = ((bf16[8,48,2048]{2,1,0:T(8,128)(2,1)}), bf16[8,48,2048]{2,1,0:T(8,128)(2,1)}, u32[]{:S(2)}, u32[]{:S(2)}) async-start(bf16[8,48,2048]{2,1,0:T(8,128)(2,1)} %broadcast_select_fusion), calls=%async_computation | async-start | bytes 3145728 | tf_op jit(solution)/shard_map/all_to_all | solution.py:164
  34.8 31.8 %all-to-all-done = bf16[8,48,2048]{2,1,0:T(8,128)(2,1)} async-done(((bf16[8,48,2048]{2,1,0:T(8,128)(2,1)}), bf16[8,48,2048]{2,1,0:T(8,128)(2,1)}, u32[]{:S(2)}, u32[]{:S(2)}) %all-to-all-start) | async-done | bytes 1572896 | tf_op jit(solution)/shard_map/all_to_all | solution.py:164
  66.7 4.3 %all-to-all-start.1 = ((bf16[8,48,2048]{2,1,0:T(8,128)(2,1)}), bf16[8,48,2048]{2,1,0:T(8,128)(2,1)}, u32[]{:S(2)}, u32[]{:S(2)}) async-start(bf16[8,48,2048]{2,1,0:T(8,128)(2,1)} %fusion.2), calls=%async_computation.1 | async-start | bytes 3145728 | tf_op jit(solution)/shard_map/all_to_all | solution.py:163
  71.1 3.4 %fusion.13 = f32[384,512]{1,0:T(8,128)} fusion(bf16[384,2048]{1,0:T(8,128)(2,1)} %bitcast.5, bf16[1,512,2048]{2,1,0:T(8,128)(2,1)S(1)} %copy-done), kind=kOutput, calls=%fused_computation.28 | convolution fusion | flops 805306368 | bytes 4456448 | tf_op jit(solution)/shard_map/vmap()/dot_general | solution.py:73
  74.5 3.4 %fusion.7 = f32[384,512]{1,0:T(8,128)} fusion(bf16[384,2048]{1,0:T(8,128)(2,1)} %bitcast.5, bf16[1,512,2048]{2,1,0:T(8,128)(2,1)S(1)} %copy-done.8), kind=kOutput, calls=%fused_computation.22 | convolution fusion | flops 805306368 | bytes 4456448 | tf_op jit(solution)/shard_map/vmap()/dot_general | solution.py:74
  77.9 30.9 %all-to-all-done.1 = bf16[8,48,2048]{2,1,0:T(8,128)(2,1)} async-done(((bf16[8,48,2048]{2,1,0:T(8,128)(2,1)}), bf16[8,48,2048]{2,1,0:T(8,128)(2,1)}, u32[]{:S(2)}, u32[]{:S(2)}) %all-to-all-start.1) | async-done | bytes 1572896 | tf_op jit(solution)/shard_map/all_to_all | solution.py:163
  108.8 3.9 %select_convert_fusion = (bf16[384,512]{1,0:T(8,128)(2,1)S(1)}, bf16[384,512]{1,0:T(8,128)(2,1)S(1)}) fusion(f32[384,512]{1,0:T(8,128)} %fusion.7, f32[384,512]{1,0:T(8,128)} %fusion.13, bf16[384,2048]{1,0:T(8,128)(2,1)} %bitcast.8, bf16[1,512,2048]{2,1,0:T(8,128)(2,1)} %param.31), kind=kOutput, calls=%fused_computation.55 | convolution fusion | flops 809631744 | bytes 6029312 | tf_op jit(solution)/shard_map/vmap()/dot_general | solution.py:79
  130.7 13.4 %all_gather.25 = f32[8,4,4]{2,1,0:T(4,128)S(1)} all-gather(f32[1,4,4]{2,1,0:T(4,128)} %exp.173), channel_id=1, replica_groups=mesh['sp'=8,'tp'=4] {'sp'}, dimensions={0}, use_global_device_ids=true | all-gather | bytes 576 | tf_op jit(solution)/shard_map/all_gather | solution.py:17
  147.0 4.6 %all-to-all-start.2 = ((bf16[8,48,512]{2,1,0:T(8,128)(2,1)}), bf16[8,48,512]{2,1,0:T(8,128)(2,1)}, u32[]{:S(2)}, u32[]{:S(2)}) async-start(bf16[8,48,512]{2,1,0:T(8,128)(2,1)} %bitcast.177), calls=%async_computation.3 | async-start | bytes 786432 | tf_op jit(solution)/shard_map/all_to_all | solution.py:182
  155.5 18.7 %all-to-all-done.2 = bf16[8,48,512]{2,1,0:T(8,128)(2,1)} async-done(((bf16[8,48,512]{2,1,0:T(8,128)(2,1)}), bf16[8,48,512]{2,1,0:T(8,128)(2,1)}, u32[]{:S(2)}, u32[]{:S(2)}) %all-to-all-start.2) | async-done | bytes 393248 | tf_op jit(solution)/shard_map/all_to_all | solution.py:182
  176.2 3.1 gather_fusion.3
  184.9 10.0 %all_gather.24 = bf16[128,2048]{1,0:T(8,128)(2,1)S(1)} all-gather(bf16[128,512]{1,0:T(8,128)(2,1)S(1)} %add_convert_fusion.1), channel_id=1, replica_groups=mesh['sp'=8,'tp'=4] {'tp'}, dimensions={1}, use_global_device_ids=true | all-gather | bytes 655360 | tf_op jit(solution)/shard_map/all_gather | solution.py:196
  194.9 9.7 %while.24 = (s32[]{:T(128)}, f32[4,4,64,128]{3,2,1,0:T(8,128)S(1)}, s32[]{:T(128)}, f32[8,4,4]{2,1,0:T(4,128)S(1)}, f32[8,4,4,64,128]{4,3,2,1,0:T(8,128)}, /*index=5*/s32[]{:T(128)}, s32[]{:T(128)}) while((s32[]{:T(128)}, f32[4,4,64,128]{3,2,1,0:T(8,128)S(1)}, s32[]{:T(128)}, f32[8,4,4]{2,1,0:T(4,128)S(1)}, ...), condition=%wide.region_9.10_spmd.clone, body=%wide.region_8.9_spmd.clone.sunk | while | flops 524292 | bytes 1573161 | solution.py:28
  206.4 17.1 %all-gather.6.cloned.1.call-done = bf16[2048,1024]{1,0:T(8,128)(2,1)} async-done(((bf16[256,1024]{1,0:T(8,128)(2,1)}), bf16[2048,1024]{1,0:T(8,128)(2,1)}) %all-gather.6.cloned.1.call-update) | async-done | bytes 4194320 | tf_op jit(solution)/shard_map/all_gather | solution.py:230
  223.5 4.1 %fusion.96 = f32[128,1024]{0,1:T(8,128)S(1)} fusion(bf16[128,2048]{1,0:T(8,128)(2,1)S(1)} %all_gather.24, bf16[2048,1024]{1,0:T(8,128)(2,1)} %all-gather.6.cloned.1.call-done), kind=kOutput, calls=%fused_computation.170 | convolution fusion | flops 536870912 | bytes 5242880 | tf_op jit(solution)/shard_map/dot_general | solution.py:228
  227.7 3.8 %multiply_reduce_fusion.3 = (f32[128,4,4]{0,2,1:T(4,128)}, f32[128,4,4]{0,2,1:T(4,128)}, f32[128,4,4,64]{0,3,2,1:T(8,128)S(1)}, bf16[128,4,4,64]{0,3,2,1:T(8,128)(2,1)}, bf16[128,4,4,64]{0,3,2,1:T(8,128)(2,1)}) fusion(f32[128,4,4,64]{0,3,2,1:T(8,128)S(1)} %copy-done.15, f32[128,4,4,64]{0,3,2,1:T(8,128)S(1)} %copy-done.17, ...), kind=kOutput, calls=%fused_computation.71 | convolution fusion | flops 205385728 | bytes 3989504 | tf_op jit(solution)/shard_map/jvp()/while/body/eval_jaxpr/grls,sgrp->lgrp/dot_general | solution.py:44
  233.7 4.3 %convolution_convert_fusion = bf16[2048,1024]{1,0:T(8,128)(2,1)} fusion(bf16[128,2048]{1,0:T(8,128)(2,1)S(1)} %all_gather.24, bf16[128,1024]{0,1:T(8,128)(2,1)} %bitcast.178), kind=kOutput, calls=%fused_computation.11 | convolution fusion | flops 538968064 | bytes 4980736 | tf_op jit(solution)/shard_map/dot_general | solution.py:247
  238.0 4.3 %fusion.4 = bf16[1,512,2048]{2,1,0:T(8,128)(2,1)} fusion(bf16[384,512]{1,0:T(8,128)(2,1)} %copy-done.14, bf16[384,2048]{1,0:T(8,128)(2,1)} %bitcast.5), kind=kOutput, calls=%fused_computation.19 | convolution fusion | flops 806354944 | bytes 4063232 | tf_op jit(solution)/shard_map/vmap()/dot_general | solution.py:97
  242.3 4.1 %fusion.3 = bf16[1,512,2048]{2,1,0:T(8,128)(2,1)} fusion(bf16[384,512]{1,0:T(8,128)(2,1)S(1)} %copy-done.19, bf16[384,2048]{1,0:T(8,128)(2,1)} %bitcast.5), kind=kOutput, calls=%fused_computation.18 | convolution fusion | flops 806354944 | bytes 4063232 | tf_op jit(solution)/shard_map/vmap()/dot_general | solution.py:94
  246.5 4.2 %fusion.5 = bf16[1,512,2048]{2,1,0:T(8,128)(2,1)} fusion(bf16[384,2048]{1,0:T(8,128)(2,1)} %bitcast.8, f32[384,512]{1,0:T(8,128)S(1)} %copy-done.41, f32[384,512]{1,0:T(8,128)S(1)} %copy-done.42), kind=kOutput, calls=%fused_computation.20 | convolution fusion | flops 808321024 | bytes 5242880 | tf_op jit(solution)/shard_map/vmap()/dot_general | solution.py:91
  258.8 20.3 %all-gather.10.cloned.1.call-done = f32[32,4,64,128]{3,2,1,0:T(8,128)} async-done(((f32[4,4,64,128]{3,2,1,0:T(8,128)}), f32[32,4,64,128]{3,2,1,0:T(8,128)}) %all-gather.10.cloned.1.call-update) | async-done | bytes 4194320 | tf_op jit(solution)/shard_map/all_gather | solution.py:17
  279.1 15.2 %while.25 = (s32[]{:T(128)}, f32[4,4,64,128]{3,2,1,0:T(8,128)S(1)}, s32[]{:T(128)}, f32[8,4,4]{2,1,0:T(4,128)}, f32[8,4,4,64,128]{4,3,2,1,0:T(8,128)}, /*index=5*/s32[]{:T(128)}, s32[]{:T(128)}, s32[]{:T(128)}, s32[]{:T(128)}) while((s32[]{:T(128)}, f32[4,4,64,128]{3,2,1,0:T(8,128)S(1)}, s32[]{:T(128)}, f32[8,4,4]{2,1,0:T(4,128)}, ...), condition=%wide.region_12.13_spmd.clone, body=%wide.region_11.12_spmd.clone.sunk | while | flops 524296 | bytes 1573223 | solution.py:28
  294.8 3.4 multiply_reduce_fusion.4
  307.3 22.8 %reduce-scatter.5.cloned.1.call-done = bf16[256,1024]{1,0:T(8,128)(2,1)} async-done(((bf16[2048,1024]{1,0:T(8,128)(2,1)}), bf16[256,1024]{1,0:T(8,128)(2,1)}) %reduce-scatter.5.cloned.1.call-update) | async-done | bytes 524304 | tf_op jit(solution)/shard_map/reduce_scatter | solution.py:246
  (216 shorter events, 100.3 us)
Async XLA Ops:
  8.0 63.0 %copy-start = (bf16[1,512,2048]{2,1,0:T(8,128)(2,1)S(1)}, bf16[1,512,2048]{2,1,0:T(8,128)(2,1)}, u32[]{:S(2)}) copy-start(bf16[1,512,2048]{2,1,0:T(8,128)(2,1)} %param.29) | copy-start | bytes 6291460
  8.0 8.4 %copy-start.2 = (bf16[128,2048]{1,0:T(8,128)(2,1)S(1)}, bf16[128,2048]{1,0:T(8,128)(2,1)}, u32[]{:S(2)}) copy-start(bf16[128,2048]{1,0:T(8,128)(2,1)} %param.25) | copy-start | bytes 1572868
  22.3 6.6 %copy-start.1 = (bf16[128,2048]{1,0:T(8,128)(2,1)S(1)}, bf16[128,2048]{1,0:T(8,128)(2,1)}, u32[]{:S(2)}) copy-start(bf16[128,2048]{1,0:T(8,128)(2,1)} %param.26) | copy-start | bytes 1572868
  22.3 44.4 %all-to-all-start = ((bf16[8,48,2048]{2,1,0:T(8,128)(2,1)}), bf16[8,48,2048]{2,1,0:T(8,128)(2,1)}, u32[]{:S(2)}, u32[]{:S(2)}) async-start(bf16[8,48,2048]{2,1,0:T(8,128)(2,1)} %broadcast_select_fusion), calls=%async_computation | async-start | bytes 3145728 | tf_op jit(solution)/shard_map/all_to_all | solution.py:164
  66.7 42.1 %all-to-all-start.1 = ((bf16[8,48,2048]{2,1,0:T(8,128)(2,1)}), bf16[8,48,2048]{2,1,0:T(8,128)(2,1)}, u32[]{:S(2)}, u32[]{:S(2)}) async-start(bf16[8,48,2048]{2,1,0:T(8,128)(2,1)} %fusion.2), calls=%async_computation.1 | async-start | bytes 3145728 | tf_op jit(solution)/shard_map/all_to_all | solution.py:163
  71.0 76.0 %reduce-scatter.3.cloned.1.call-start = ((), (), s32[]{:S(2)}) async-start(), calls=%async_computation.5 | async-start | bytes 1966080 | tf_op jit(solution)/shard_map/reduce_scatter | solution.py:176
  116.8 78.1 %all-gather.8.cloned.1.call-start = ((), (), s32[]{:S(2)}) async-start(), calls=%async_computation.8 | async-start | bytes 4718592 | tf_op jit(solution)/shard_map/all_gather | solution.py:17
  118.5 4.4 %copy-start.5 = (f32[128,1024]{0,1:T(8,128)}, f32[128,1024]{0,1:T(8,128)S(1)}, u32[]{:S(2)}) copy-start(f32[128,1024]{0,1:T(8,128)S(1)} %copy.156) | copy-start | bytes 1572868
  119.6 7.4 %copy-start.10 = (bf16[128,4,128]{2,1,0:T(4,128)(2,1)}, bf16[128,4,128]{2,1,0:T(4,128)(2,1)S(1)}, u32[]{:S(2)}) copy-start(bf16[128,4,128]{2,1,0:T(4,128)(2,1)S(1)} %squeeze.133) | copy-start | bytes 393220
  122.3 101.2 %all-gather.6.cloned.1.call-start = ((), (), s32[]{:S(2)}) async-start(), calls=%async_computation.7 | async-start | bytes 4718592 | tf_op jit(solution)/shard_map/all_gather | solution.py:230
  147.0 27.3 %all-to-all-start.2 = ((bf16[8,48,512]{2,1,0:T(8,128)(2,1)}), bf16[8,48,512]{2,1,0:T(8,128)(2,1)}, u32[]{:S(2)}, u32[]{:S(2)}) async-start(bf16[8,48,512]{2,1,0:T(8,128)(2,1)} %bitcast.177), calls=%async_computation.3 | async-start | bytes 786432 | tf_op jit(solution)/shard_map/all_to_all | solution.py:182
  151.6 127.5 %all-gather.10.cloned.1.call-start = ((), (), s32[]{:S(2)}) async-start(), calls=%async_computation.9 | async-start | bytes 4718592 | tf_op jit(solution)/shard_map/all_gather | solution.py:17
  152.5 99.9 %copy-start.28 = (pred[128,128]{1,0:T(8,128)(4,1)}, pred[128,128]{1,0:T(8,128)(4,1)S(1)}, u32[]{:S(2)}) copy-start(pred[128,128]{1,0:T(8,128)(4,1)S(1)} %iota_compare_fusion) | copy-start | bytes 49156
  206.4 21.2 %copy-start.23 = (f32[128,4,4]{0,2,1:T(4,128)S(1)}, f32[128,4,4]{0,2,1:T(4,128)}, u32[]{:S(2)}) copy-start(f32[128,4,4]{0,2,1:T(4,128)} %get-tuple-element.689) | copy-start | bytes 24580
  206.4 21.2 %copy-start.25 = (f32[128,16]{0,1:T(8,128)S(1)}, f32[128,16]{0,1:T(8,128)}, u32[]{:S(2)}) copy-start(f32[128,16]{0,1:T(8,128)} %param.22) | copy-start | bytes 24580
  206.4 21.2 %copy-start.32 = (f32[4,4,128]{2,1,0:T(4,128)S(1)}, f32[4,4,128]{2,1,0:T(4,128)}, u32[]{:S(2)}) copy-start(f32[4,4,128]{2,1,0:T(4,128)} %copy.160) | copy-start | bytes 24580
  233.5 96.6 %reduce-scatter.5.cloned.1.call-start = ((), (), s32[]{:S(2)}) async-start(), calls=%async_computation.6 | async-start | bytes 4718592 | tf_op jit(solution)/shard_map/reduce_scatter | solution.py:246
  279.1 15.2 %copy-start.11 = (bf16[128,4,128]{2,1,0:T(4,128)(2,1)S(1)}, bf16[128,4,128]{2,1,0:T(4,128)(2,1)}, u32[]{:S(2)}) copy-start(bf16[128,4,128]{2,1,0:T(4,128)(2,1)} %copy-done.10) | copy-start | bytes 393220
  279.1 15.6 %copy-start.26 = (f32[128,16]{0,1:T(8,128)S(1)}, f32[128,16]{0,1:T(8,128)}, u32[]{:S(2)}) copy-start(f32[128,16]{0,1:T(8,128)} %param.22) | copy-start | bytes 24580
  279.1 15.6 %copy-start.29 = (pred[128,128]{1,0:T(8,128)(4,1)S(1)}, pred[128,128]{1,0:T(8,128)(4,1)}, u32[]{:S(2)}) copy-start(pred[128,128]{1,0:T(8,128)(4,1)} %copy-done.28) | copy-start | bytes 49156
  279.1 15.6 %copy-start.33 = (f32[4,4,128]{2,1,0:T(4,128)S(1)}, f32[4,4,128]{2,1,0:T(4,128)}, u32[]{:S(2)}) copy-start(f32[4,4,128]{2,1,0:T(4,128)} %copy.160) | copy-start | bytes 24580
  294.8 6.8 %copy-start.31 = (f32[16]{0:T(128)S(1)}, f32[16]{0:T(128)}, u32[]{:S(2)}) copy-start(f32[16]{0:T(128)} %param.23) | copy-start | bytes 196
  294.8 6.8 %copy-start.40 = (f32[16]{0:T(128)S(1)}, f32[16]{0:T(128)}, u32[]{:S(2)}) copy-start(f32[16]{0:T(128)} %copy-done.39) | copy-start | bytes 196
  298.6 7.8 %copy-start.22 = (bf16[128,4,4,64]{0,3,2,1:T(8,128)(2,1)S(1)}, bf16[128,4,4,64]{0,3,2,1:T(8,128)(2,1)}, u32[]{:S(2)}) copy-start(bf16[128,4,4,64]{0,3,2,1:T(8,128)(2,1)} %get-tuple-element.685) | copy-start | bytes 786436
  (27 other events, 76.5 us)
Sparse Core Ops, SparseCore 0:
  116.9 30.0 reduce-scatter.2
Sparse Core Ops, SparseCore 1:
  122.3 54.2 all-gather.7
  178.0 45.4 all-gather.5
  233.5 45.5 all-gather.9
  281.4 48.6 reduce-scatter.4
where the time goes:
time: 342 us; the launch traced here: 340 us
  waiting for transfers between devices  145 us (42%)
  matrix products  58.1 us (17%)
  local copies, waits for them, and re-layouts  41.1 us (12%)
  other arithmetic  38.9 us (11%)
  blocking collectives  23.4 us (7%)
  between operations  16.3 us (5%)
  starting transfers between devices  16 us (5%)
    all_to_all x1, waiting for transfers between devices, body(): lax.all_to_all(send_rows, 'sp', split_axis=0, concat_axis=0, tiled=True)  31.8 us
    all_to_all x1, waiting for transfers between devices, body(): lax.all_to_all(send_grad, 'sp', split_axis=0, concat_axis=0, tiled=True)  30.9 us
    reduce_scatter x1, waiting for transfers between devices, body(): lax.psum_scatter(lax.dot_general(stream_part_cols, gated_out, across, pre...  22.8 us
    all_gather x2, waiting for transfers between devices, prefix(): everything = jax.tree.map(lambda part: lax.all_gather(part, axis), x)  20.3 us
    select_n x16, other arithmetic, lap(): return jax.tree.map(lambda a, b: jnp.where(reached, a, b), new, before)  18.8 us
    all_to_all x1, waiting for transfers between devices, body(): lax.all_to_all(reduced.reshape(all_experts, capacity, col_width).astype(j...  18.7 us
    all_gather x1, waiting for transfers between devices, body(): lax.all_gather(out_proj, 'sp', axis=0, tiled=True)  17.1 us
    all_gather x1, blocking collectives, prefix(): everything = jax.tree.map(lambda part: lax.all_gather(part, axis), x)  13.4 us
  transfers between devices with their start and end apart: 8, of which 7 were waited for; matrix products, arithmetic and copies ran while one was open for 30% of the time, Pallas kernels for 0%

commit v1 on v0

v1 whole, which is shorter than its diff:
```python
import functools

import jax
import jax.numpy as jnp
from jax import lax
from jax.experimental import pallas as pl
from jax.experimental.pallas import tpu as pltpu
from jax.sharding import PartitionSpec as P

NSTATE = 128
CLAMP_LIMIT = 7.0
SIGMOID_SCALE = 1.702
HIGHEST = lax.Precision.HIGHEST
F32 = jnp.float32
BF16 = jnp.bfloat16
NN = (((1,), (0,)), ((), ()))
NT = (((1,), (1,)), ((), ()))
TN = (((0,), (0,)), ((), ()))


def mm(a, b, dims=NN):
    return lax.dot_general(a, b, dims, preferred_element_type=F32)


def mm_exact(a, b, dims=NN):
    return lax.dot_general(a, b, dims, precision=HIGHEST, preferred_element_type=F32)


def grid_of(rows, cols):
    return (
        lax.broadcasted_iota(jnp.int32, (rows, cols), 0),
        lax.broadcasted_iota(jnp.int32, (rows, cols), 1),
    )


def spread(heads, size):
    at, col = grid_of(heads, heads * size)
    return ((col >= at * size) & (col < (at + 1) * size)).astype(F32)


def fold(heads, size):
    col, at = grid_of(heads * size, heads)
    return ((col >= at * size) & (col < (at + 1) * size)).astype(F32)


def call(kernel, outs, flops, *args, vmem=None):
    bytes_accessed = sum(a.size * a.dtype.itemsize for a in args)
    bytes_accessed += sum(o.size * o.dtype.itemsize for o in outs)
    return pl.pallas_call(
        kernel,
        out_shape=outs,
        in_specs=[pl.BlockSpec(memory_space=pltpu.VMEM)] * len(args),
        out_specs=[pl.BlockSpec(memory_space=pltpu.VMEM)] * len(outs),
        cost_estimate=pl.CostEstimate(
            flops=flops, bytes_accessed=bytes_accessed, transcendentals=0
        ),
        compiler_params=pltpu.CompilerParams(vmem_limit_bytes=vmem or 24 * 2**20),
    )(*args)


def out(shape, dtype):
    return jax.ShapeDtypeStruct(shape, dtype)


def dispatch_kernel(experts, cap, width, routes_ref, weights_ref, x_ref, g_ref, xs_ref, gs_ref, sel_ref):
    tokens, top = routes_ref.shape
    start = pl.multiple_of(lax.axis_index("tp") * width, 128)
    x = x_ref[:, pl.ds(start, width)]
    g = g_ref[:, pl.ds(start, width)].astype(F32)
    _, expert = grid_of(tokens, experts)
    _, slot = grid_of(tokens, experts * cap)
    row, col = grid_of(tokens, tokens)
    hits = [expert == routes_ref[:, k : k + 1] for k in range(top)]
    named = sum(hit.astype(F32) for hit in hits)
    before = mm((row > col).astype(BF16), named.astype(BF16))
    every = jnp.zeros((tokens, experts * cap), F32)
    grads = jnp.zeros((experts * cap, width), F32)
    for k in range(top):
        rank = jnp.sum(jnp.where(hits[k], before, 0.0), axis=1, keepdims=True).astype(jnp.int32)
        chosen = (slot == routes_ref[:, k : k + 1] * cap + rank).astype(F32)
        every = every + chosen
        grads = grads + mm(chosen.astype(BF16), (g * weights_ref[:, k : k + 1]).astype(BF16), TN)
    picked = every.astype(BF16)
    sel_ref[...] = picked
    xs_ref[...] = mm(picked, x, TN).astype(BF16)
    gs_ref[...] = grads.astype(BF16)


def combine_kernel(width, sel_ref, back_ref, g_ref, out_ref):
    start = pl.multiple_of(lax.axis_index("tp") * width, 128)
    g = g_ref[:, pl.ds(start, width)].astype(F32)
    out_ref[...] = (g + mm(sel_ref[...], back_ref[...])).astype(BF16)


def mixing_of(log_ref, logt_ref, h):
    length = log_ref.shape[0]
    row, col = grid_of(length, length)
    gap = log_ref[:, h : h + 1] - logt_ref[h : h + 1, :]
    return jnp.where(row >= col, jnp.exp(jnp.minimum(gap, 0.0)), 0.0)


def local_kernel(groups, v_ref, b_ref, c_ref, steps_ref, log_ref, logt_ref, y_ref, state_ref):
    heads = steps_ref.shape[1]
    per, size = heads // groups, v_ref.shape[1] // heads
    wide = per * size
    length = v_ref.shape[0]
    expand = spread(heads, size)
    to_end = jnp.exp(log_ref[length - 1 :, :] - log_ref[...])
    x = v_ref[...].astype(F32) * mm_exact(steps_ref[...], expand)
    xe = (x * mm_exact(to_end, expand)).astype(BF16)
    x = x.astype(BF16)
    for g in range(groups):
        keys = b_ref[:, g * NSTATE : (g + 1) * NSTATE]
        scores = mm(c_ref[:, g * NSTATE : (g + 1) * NSTATE], keys, NT)
        parts = []
        for r in range(per):
            h = g * per + r
            att = (scores * mixing_of(log_ref, logt_ref, h)).astype(BF16)
            parts.append(mm(att, x[:, h * size : (h + 1) * size]))
        y_ref[:, g * wide : (g + 1) * wide] = jnp.concatenate(parts, axis=1)
        state_ref[g] = mm(xe[:, g * wide : (g + 1) * wide], keys, TN).astype(BF16)


def weighted_state(all_ref, weights_ref, g, r, per, size):
    h = g * per + r
    total = jnp.zeros((size, NSTATE), F32)
    for j in range(all_ref.shape[0]):
        part = all_ref[j, g, r * size : (r + 1) * size, :].astype(F32)
        total = total + weights_ref[j : j + 1, h : h + 1] * part
    return total


def enter_kernel(groups, all_ref, weights_ref, y_ref, gate_ref, c_ref, log_ref, out_ref, gated_ref, state_ref):
    heads = log_ref.shape[1]
    per, size = heads // groups, y_ref.shape[1] // heads
    wide = per * size
    decay = mm_exact(jnp.exp(log_ref[...]), spread(heads, size))
    for g in range(groups):
        state = jnp.concatenate(
            [weighted_state(all_ref, weights_ref, g, r, per, size) for r in range(per)], axis=0
        ).astype(BF16)
        state_ref[g] = state
        at = slice(g * wide, (g + 1) * wide)
        entered = mm(c_ref[:, g * NSTATE : (g + 1) * NSTATE], state, NT) * decay[:, at]
        mixed = y_ref[:, at] + entered
        out_ref[:, at] = mixed
        gate = gate_ref[:, at].astype(F32)
        gated_ref[:, at] = (mixed * gate * jax.nn.sigmoid(gate)).astype(BF16)


def gate_kernel(groups, grad_ref, out_ref, gate_ref, c_ref, log_ref, gate_grad_ref, mixer_ref, state_ref):
    heads = log_ref.shape[1]
    wide = grad_ref.shape[1] // groups
    decay = mm_exact(jnp.exp(log_ref[...]), spread(heads, grad_ref.shape[1] // heads))
    for g in range(groups):
        at = slice(g * wide, (g + 1) * wide)
        gate = gate_ref[:, at].astype(F32)
        sig = jax.nn.sigmoid(gate)
        grad = grad_ref[:, at]
        gate_grad_ref[:, at] = (grad * out_ref[:, at] * sig * (1.0 + gate * (1.0 - sig))).astype(BF16)
        mixer = grad * gate * sig
        mixer_ref[:, at] = mixer
        keys = c_ref[:, g * NSTATE : (g + 1) * NSTATE]
        state_ref[g] = mm((mixer * decay[:, at]).astype(BF16), keys, TN).astype(BF16)


def inner_kernel(
    groups, v_ref, b_ref, c_ref, steps_ref, log_ref, logt_ref, mixer_ref, state_ref,
    out_keys_ref, in_part_ref, x_part_ref, base_ref,
):
    heads = steps_ref.shape[1]
    per, size = heads // groups, v_ref.shape[1] // heads
    wide = per * size
    length = v_ref.shape[0]
    row, col = grid_of(length, length)
    later = (row <= col).astype(BF16)
    expand = spread(heads, size)
    mixer = mixer_ref[...]
    decayed = mixer * mm_exact(jnp.exp(log_ref[...]), expand)
    decayed_low = decayed.astype(BF16)
    mixer = mixer.astype(BF16)
    x = (v_ref[...].astype(F32) * mm_exact(steps_ref[...], expand)).astype(BF16)
    entering = []
    _, head_at = grid_of(length, heads)
    pairs = jnp.zeros((length, heads), F32)
    for g in range(groups):
        at = slice(g * wide, (g + 1) * wide)
        keys_in = b_ref[:, g * NSTATE : (g + 1) * NSTATE]
        keys_out = c_ref[:, g * NSTATE : (g + 1) * NSTATE]
        scores = mm(keys_out, keys_in, NT)
        score_grad = jnp.zeros((length, length), F32)
        parts = []
        for r in range(per):
            h = g * per + r
            here = slice(h * size, (h + 1) * size)
            mixing = mixing_of(log_ref, logt_ref, h)
            att = scores * mixing
            att_grad = mm(mixer[:, here], x[:, here], NT)
            parts.append(mm(att.astype(BF16), mixer[:, here], TN))
            score_grad = score_grad + att_grad * mixing
            after = mm(later, (att_grad * att).astype(BF16))
            crossing = jnp.sum(jnp.where(col < row, after, 0.0), axis=1, keepdims=True)
            pairs = pairs + jnp.where(head_at == h, crossing, 0.0)
        x_part_ref[:, at] = jnp.concatenate(parts, axis=1)
        score_grad = score_grad.astype(BF16)
        state = state_ref[g]
        out_keys_ref[:, g * NSTATE : (g + 1) * NSTATE] = (
            mm(score_grad, keys_in) + mm(decayed_low[:, at], state)
        ).astype(BF16)
        in_part_ref[:, g * NSTATE : (g + 1) * NSTATE] = mm(score_grad, keys_out, TN)
        entering.append(decayed[:, at] * mm(keys_out, state, NT))
    entering = jnp.concatenate(entering, axis=1)
    sums = mm_exact(entering, fold(heads, size))
    base_ref[...] = pairs + mm_exact((row <= col).astype(F32), sums)


def outer_kernel(
    groups, all_ref, weights_ref, state_ref, v_ref, b_ref, steps_ref, log_ref, rates_ref,
    in_part_ref, x_part_ref, base_ref, values_ref, in_keys_ref, steps_grad_ref,
):
    heads = steps_ref.shape[1]
    per, size = heads // groups, v_ref.shape[1] // heads
    wide = per * size
    length = v_ref.shape[0]
    row, col = grid_of(length, length)
    expand = spread(heads, size)
    last = log_ref[length - 1 :, :]
    steps = mm_exact(steps_ref[...], expand)
    to_end = mm_exact(jnp.exp(last - log_ref[...]), expand)
    values = v_ref[...].astype(F32)
    xe = values * steps * to_end
    xe_low = xe.astype(BF16)
    leaving, direct = [], []
    _, head_at = grid_of(1, heads)
    passing = jnp.zeros((1, heads), F32)
    for g in range(groups):
        at = slice(g * wide, (g + 1) * wide)
        keys_in = b_ref[:, g * NSTATE : (g + 1) * NSTATE]
        tiles = [weighted_state(all_ref, weights_ref, g, r, per, size) for r in range(per)]
        for r in range(per):
            before = state_ref[g, r * size : (r + 1) * size, :].astype(F32)
            both = jnp.sum(jnp.sum(tiles[r] * before, axis=0, keepdims=True), axis=1, keepdims=True)
            passing = passing + jnp.where(head_at == g * per + r, both, 0.0)
        after = jnp.concatenate(tiles, axis=0).astype(BF16)
        reached = mm(keys_in, after, NT)
        x_grad = x_part_ref[:, at] + reached * to_end[:, at]
        values_ref[:, at] = (x_grad * steps[:, at]).astype(BF16)
        in_keys_ref[:, g * NSTATE : (g + 1) * NSTATE] = (
            in_part_ref[:, g * NSTATE : (g + 1) * NSTATE] + mm(xe_low[:, at], after)
        ).astype(BF16)
        leaving.append(reached * xe[:, at])
        direct.append(x_grad * values[:, at])
    gather = fold(heads, size)
    leaving = mm_exact(jnp.concatenate(leaving, axis=1), gather)
    direct = mm_exact(jnp.concatenate(direct, axis=1), gather)
    crossing = base_ref[...] + mm_exact((col < row).astype(F32), leaving) + jnp.exp(last) * passing
    steps_grad_ref[...] = direct - rates_ref[...] * crossing


def side_by_side(stacked):
    return jnp.concatenate([stacked[c] for c in range(stacked.shape[0])], axis=-1)


def body(
    mix_values,
    mix_gate,
    input_keys,
    output_keys,
    step_sizes,
    decay_rates,
    out_proj,
    expert_inputs,
    stream_grad,
    routes,
    route_weights,
    gate_proj,
    up_proj,
    down_proj,
):
    tok_rows = mix_values.shape[0]
    model_width = stream_grad.shape[1]
    top = routes.shape[1]
    sp_devices = lax.axis_size("sp")
    tp_devices = lax.axis_size("tp")
    experts = gate_proj.shape[0] * sp_devices
    cap = 3 * tok_rows * top // (2 * experts)
    slots = experts * cap
    heads = step_sizes.shape[1]
    groups = input_keys.shape[1] // NSTATE
    inner = mix_values.shape[1]
    size = inner // heads
    wide = inner // groups
    width = model_width // tp_devices
    state_shape = (groups, wide, NSTATE)
    pair_flops = 2 * tok_rows * tok_rows * inner

    send_rows, send_grad, chosen = call(
        functools.partial(dispatch_kernel, experts, cap, width),
        [out((slots, width), BF16), out((slots, width), BF16), out((tok_rows, slots), BF16)],
        6 * tok_rows * slots * width,
        routes, route_weights, expert_inputs, stream_grad,
    )

    def to_experts(rows):
        got = lax.all_to_all(
            rows.reshape(experts, cap, width), "sp", split_axis=0, concat_axis=0, tiled=True
        )
        return lax.all_gather(got.reshape(slots, width), "tp", axis=0)

    in_rows = side_by_side(to_experts(send_rows))
    grad_rows = side_by_side(to_experts(send_grad))

    row, col = grid_of(tok_rows, tok_rows)
    rates = decay_rates.reshape(1, heads)
    drop = -step_sizes * rates
    log_decay = mm_exact((row >= col).astype(F32), drop)
    log_decay_t = log_decay.T
    y_local, own_state = call(
        functools.partial(local_kernel, groups),
        [out((tok_rows, inner), F32), out(state_shape, BF16)],
        3 * pair_flops,
        mix_values, input_keys, output_keys, step_sizes, log_decay, log_decay_t,
    )
    spans = lax.all_gather(log_decay[tok_rows - 1], "sp", axis=0)
    here = lax.axis_index("sp")
    order = jnp.arange(sp_devices)
    one, two = order[:, None], order[None, :]
    forward = mm_exact(((two > one) & (two < here)).astype(F32), spans)
    forward = jnp.where(one < here, jnp.exp(forward), 0.0)
    backward = mm_exact(((two < one) & (two > here)).astype(F32), spans)
    backward = jnp.where(one > here, jnp.exp(backward), 0.0)
    all_states = lax.all_gather(own_state, "sp", axis=0)
    mixer_out, gated_out, state_in = call(
        functools.partial(enter_kernel, groups),
        [out((tok_rows, inner), F32), out((tok_rows, inner), BF16), out(state_shape, BF16)],
        2 * pair_flops,
        all_states, forward, y_local, mix_gate, output_keys, log_decay,
    )
    full_proj = lax.all_gather(out_proj, "sp", axis=0, tiled=True)
    all_gated = lax.all_gather(gated_out, "sp", axis=0, tiled=True)

    gate_weight = gate_proj.reshape(-1, model_width)
    up_weight = up_proj.reshape(-1, model_width)
    down_weight = down_proj.reshape(-1, model_width)
    gate_pre = mm(in_rows, gate_weight, NT)
    up_pre = mm(in_rows, up_weight, NT)
    gate_clamped = jnp.minimum(gate_pre, CLAMP_LIMIT)
    up_clamped = jnp.clip(up_pre, -CLAMP_LIMIT, CLAMP_LIMIT)
    gate_sigmoid = jax.nn.sigmoid(SIGMOID_SCALE * gate_clamped)
    activation = ((up_clamped + 1.0) * gate_clamped * gate_sigmoid).astype(BF16)
    act_grad = mm(grad_rows, down_weight, NT)
    gate_grad = jnp.where(
        gate_pre < CLAMP_LIMIT,
        act_grad
        * (up_clamped + 1.0)
        * gate_sigmoid
        * (1.0 + SIGMOID_SCALE * gate_clamped * (1.0 - gate_sigmoid)),
        0.0,
    ).astype(BF16)
    up_grad = jnp.where(
        jnp.abs(up_pre) < CLAMP_LIMIT, act_grad * gate_clamped * gate_sigmoid, 0.0
    ).astype(BF16)
    back = (mm(gate_grad, gate_weight) + mm(up_grad, up_weight)).astype(BF16)
    grad_down_proj = mm(activation, grad_rows, TN).astype(BF16).reshape(down_proj.shape)
    grad_gate_proj = mm(gate_grad, in_rows, TN).astype(BF16).reshape(gate_proj.shape)
    grad_up_proj = mm(up_grad, in_rows, TN).astype(BF16).reshape(up_proj.shape)

    reduced = lax.psum_scatter(back, "tp", scatter_dimension=1, tiled=True)
    returned = lax.all_to_all(
        reduced.reshape(experts, cap, width), "sp", split_axis=0, concat_axis=0, tiled=True
    ).reshape(slots, width)
    stream_part = call(
        functools.partial(combine_kernel, width),
        [out((tok_rows, width), BF16)],
        2 * tok_rows * slots * width,
        chosen, returned, stream_grad,
    )[0]
    stream_total = lax.all_gather(stream_part, "tp", axis=1, tiled=True)

    gated_grad = mm(stream_total, full_proj)
    grad_gate, mixer_grad, own_grad = call(
        functools.partial(gate_kernel, groups),
        [out((tok_rows, inner), BF16), out((tok_rows, inner), F32), out(state_shape, BF16)],
        pair_flops,
        gated_grad, mixer_out, mix_gate, output_keys, log_decay,
    )
    all_grads = lax.all_gather(own_grad, "sp", axis=0)
    share = model_width // sp_devices
    all_stream = lax.all_to_all(
        stream_total, "sp", split_axis=1, concat_axis=0, tiled=True
    ).reshape(sp_devices * tok_rows, share)
    grad_out_proj = mm(all_stream, all_gated, TN)
    grad_output_keys, in_part, x_part, base = call(
        functools.partial(inner_kernel, groups),
        [
            out(output_keys.shape, BF16),
            out(input_keys.shape, F32),
            out((tok_rows, inner), F32),
            out((tok_rows, heads), F32),
        ],
        6 * pair_flops,
        mix_values, input_keys, output_keys, step_sizes, log_decay, log_decay_t, mixer_grad, state_in,
    )
    grad_values, grad_input_keys, grad_steps = call(
        functools.partial(outer_kernel, groups),
        [
            out((tok_rows, inner), BF16),
            out(input_keys.shape, BF16),
            out((tok_rows, heads), F32),
        ],
        3 * pair_flops,
        all_grads, backward, state_in, mix_values, input_keys, step_sizes, log_decay, rates,
        in_part, x_part, base,
    )
    return (
        grad_gate_proj,
        grad_up_proj,
        grad_down_proj,
        grad_out_proj,
        grad_values,
        grad_gate,
        grad_input_keys,
        grad_output_keys,
        grad_steps,
    )


def solution(mesh):
    return jax.shard_map(
        body,
        mesh=mesh,
        in_specs=(
            P("sp", "tp"),
            P("sp", "tp"),
            P("sp", "tp"),
            P("sp", "tp"),
            P("sp", "tp"),
            P("tp"),
            P("sp", "tp"),
            P("sp", None),
            P("sp", None),
            P("sp", None),
            P("sp", None),
            P("sp", "tp", None),
            P("sp", "tp", None),
            P("sp", "tp", None),
        ),
        out_specs=(
            P("sp", "tp", None),
            P("sp", "tp", None),
            P("sp", "tp", None),
            P("sp", "tp"),
            P("sp", "tp"),
            P("sp", "tp"),
            P("sp", "tp"),
            P("sp", "tp"),
            P("sp", "tp"),
        ),
        check_vma=False,
    )
```

time: 342 us -> 296 us (0.87)
  blocking collectives: 23.4 us -> 80.9 us
  other arithmetic: 38.9 us -> 0.01 us
  matrix products: 58.1 us -> 23.2 us
  local copies, waits for them, and re-layouts: 41.1 us -> 24.7 us
  Pallas kernels: 0 us -> 12.9 us
  starting transfers between devices: 16 us -> 4.6 us
  waiting for transfers between devices: 145 us -> 134 us
    all_to_all x3 -> x1, waiting for transfers between devices: 81.5 us -> 0.01 us  [body(): lax.all_to_all(stream_total, 'sp', split_axis=1, concat_axis=0, tiled=True)]
    all_gather x3 -> x6, waiting for transfers between devices: 37.4 us -> 105 us  [the longest x2 40.8 us: to_experts(): return lax.all_gather(got.reshape(slots, width), 'tp', axis=0)]
    all_to_all x0 -> x3, blocking collectives: none -> 58.3 us  [the longest x2 34.4 us: to_experts(): lax.all_to_all(rows.reshape(experts, cap, width), 'sp', split_axis=0, con...]
    dot_general x24 -> x13, matrix products: 58.1 us -> 23.2 us  [the longest x10 22.8 us: mm(): return lax.dot_general(a, b, dims, preferred_element_type=F32)]
    select_n x19 -> x0, other arithmetic: 21.6 us -> none  [the longest x16 18.8 us: lap(): return jax.tree.map(lambda a, b: jnp.where(reached, a, b), new, before)]
    pallas_call x0 -> x7, Pallas kernels: none -> 12.9 us  [call(): pl.pallas_call(kernel, out_shape=outs, in_specs=[pl.BlockSpec(memory_spac...]
    gather x4 -> x0, local copies, waits for them, and re-layouts: 12.2 us -> none  [the longest x1 3.13 us: body(): returned.reshape(all_experts * capacity, col_width)[slot_index]]
    all_to_all x3 -> x1, starting transfers between devices: 15.4 us -> 4.32 us  [body(): lax.all_to_all(stream_total, 'sp', split_axis=1, concat_axis=0, tiled=True)]
  transfers between devices with their start and end apart: 8 -> 8, of which waited for: 7 -> 7; matrix products, arithmetic and copies ran while one was open for 30% -> 10% of each run, Pallas kernels for 0% -> 3%
where the time goes in v1:
time: 296 us; the launch traced here: 295 us
  waiting for transfers between devices  134 us (45%)
  blocking collectives  80.9 us (27%)
  local copies, waits for them, and re-layouts  24.7 us (8%)
  matrix products  23.2 us (8%)
  between operations  14.7 us (5%)
  Pallas kernels  12.9 us (4%)
  starting transfers between devices  4.6 us (2%)
    all_gather x2, waiting for transfers between devices, to_experts(): return lax.all_gather(got.reshape(slots, width), 'tp', axis=0)  40.8 us
    all_to_all x2, blocking collectives, to_experts(): lax.all_to_all(rows.reshape(experts, cap, width), 'sp', split_axis=0, con...  34.4 us
    reduce_scatter x1, waiting for transfers between devices, body(): reduced = lax.psum_scatter(back, 'tp', scatter_dimension=1, tiled=True)  28.1 us
    all_gather x1, waiting for transfers between devices, body(): all_grads = lax.all_gather(own_grad, 'sp', axis=0)  26.2 us
    all_to_all x1, blocking collectives, body(): lax.all_to_all(reduced.reshape(experts, cap, width), 'sp', split_axis=0,...  23.9 us
    dot_general x10, matrix products, mm(): return lax.dot_general(a, b, dims, preferred_element_type=F32)  22.8 us
    unnamed x110, local copies, waits for them, and re-layouts  18.6 us
    all_gather x1, waiting for transfers between devices, body(): full_proj = lax.all_gather(out_proj, 'sp', axis=0, tiled=True)  17 us
  transfers between devices with their start and end apart: 8, of which 7 were waited for; matrix products, arithmetic and copies ran while one was open for 10% of the time, Pallas kernels for 3%

profile of v1, /device:TPU:0, one launch (start us, length us, event | category | flops | bytes accessed | tf_op | source)
XLA Modules:
  0.0 295.0 jit_solution(14077205488768782801)
XLA Ops:
  12.1 18.8 %all_to_all.34 = bf16[8,48,512]{2,1,0:T(8,128)(2,1)} all-to-all(bf16[8,48,512]{2,1,0:T(8,128)(2,1)S(1)} %bitcast.70), channel_id=1, replica_groups=mesh['sp'=8,'tp'=4] {'sp'}, dimensions={0} | all-to-all | bytes 786432 | tf_op jit(solution)/shard_map/all_to_all | solution.py:305
  30.9 15.6 %all_to_all.35 = bf16[8,48,512]{2,1,0:T(8,128)(2,1)} all-to-all(bf16[8,48,512]{2,1,0:T(8,128)(2,1)S(1)} %bitcast.69), channel_id=1, replica_groups=mesh['sp'=8,'tp'=4] {'sp'}, dimensions={0} | all-to-all | bytes 786432 | tf_op jit(solution)/shard_map/all_to_all | solution.py:305
  47.1 2.5 shard_map.207
  50.4 10.5 %all-gather.10.cloned.1.call-done = bf16[4,384,512]{2,1,0:T(8,128)(2,1)} async-done(((bf16[1,384,512]{2,1,0:T(8,128)(2,1)}), bf16[4,384,512]{2,1,0:T(8,128)(2,1)}) %all-gather.10.cloned.1.call-update) | async-done | bytes 1572880 | tf_op jit(solution)/shard_map/all_gather | solution.py:308
  60.9 2.4 slice_bitcast_fusion.7
  63.3 30.3 %all-gather.12.cloned.1.call-done = bf16[4,384,512]{2,1,0:T(8,128)(2,1)} async-done(((bf16[1,384,512]{2,1,0:T(8,128)(2,1)}), bf16[4,384,512]{2,1,0:T(8,128)(2,1)}) %all-gather.12.cloned.1.call-update) | async-done | bytes 1572880 | tf_op jit(solution)/shard_map/all_gather | solution.py:308
  101.7 2.2 add_convert_fusion
  104.7 12.0 %all-gather.2 = f32[8,1,16]{2,1,0:T(1,128)S(1)} all-gather(f32[1,1,16]{2,1,0:T(1,128)S(1)} %bitcast.80), channel_id=1, replica_groups=mesh['sp'=8,'tp'=4] {'sp'}, dimensions={0}, use_global_device_ids=true | all-gather | bytes 576 | tf_op jit(solution)/shard_map/all_gather | solution.py:324
  117.4 7.6 %all-gather.18.cloned.1.call-done = bf16[32,256,128]{2,1,0:T(8,128)(2,1)} async-done(((bf16[4,256,128]{2,1,0:T(8,128)(2,1)}), bf16[32,256,128]{2,1,0:T(8,128)(2,1)}) %all-gather.18.cloned.1.call-update) | async-done | bytes 2097168 | tf_op jit(solution)/shard_map/all_gather | solution.py:332
  130.8 28.1 %reduce-scatter.2.cloned.1.call-done = bf16[384,512]{1,0:T(8,128)(2,1)} async-done(((bf16[384,2048]{1,0:T(8,128)(2,1)}), bf16[384,512]{1,0:T(8,128)(2,1)}) %reduce-scatter.2.cloned.1.call-update) | async-done | bytes 393232 | tf_op jit(solution)/shard_map/reduce_scatter | solution.py:368
  159.0 23.9 %all_to_all.36 = bf16[8,48,512]{2,1,0:T(8,128)(2,1)S(1)} all-to-all(bf16[8,48,512]{2,1,0:T(8,128)(2,1)} %bitcast.77), channel_id=1, replica_groups=mesh['sp'=8,'tp'=4] {'sp'}, dimensions={0} | all-to-all | bytes 786432 | tf_op jit(solution)/shard_map/all_to_all | solution.py:369
  184.0 10.6 %all_gather.32 = bf16[128,2048]{1,0:T(8,128)(2,1)} all-gather(bf16[128,512]{1,0:T(8,128)(2,1)S(1)} %shard_map.206), channel_id=1, replica_groups=mesh['sp'=8,'tp'=4] {'tp'}, dimensions={1}, use_global_device_ids=true | all-gather | bytes 655360 | tf_op jit(solution)/shard_map/all_gather | solution.py:378
  194.7 17.0 %all-gather.16.cloned.1.call-done = bf16[2048,1024]{1,0:T(8,128)(2,1)} async-done(((bf16[256,1024]{1,0:T(8,128)(2,1)}), bf16[2048,1024]{1,0:T(8,128)(2,1)}) %all-gather.16.cloned.1.call-update) | async-done | bytes 4194320 | tf_op jit(solution)/shard_map/all_gather | solution.py:339
  211.7 3.1 %fusion.35.grad_ref = f32[128,1024]{1,0:T(8,128)S(1)} fusion(bf16[128,2048]{1,0:T(8,128)(2,1)} %all_gather.32, bf16[2048,1024]{1,0:T(8,128)(2,1)} %all-gather.16.cloned.1.call-done), kind=kOutput, calls=%fused_computation.62 | convolution fusion | flops 536870912 | bytes 5242880 | tf_op jit(solution)/shard_map/dot_general | solution.py:22
  217.7 1.9 copy.60
  219.6 4.3 %all-to-all-start.3 = ((bf16[128,8,256]{2,0,1:T(8,128)(2,1)}), bf16[128,8,256]{2,0,1:T(8,128)(2,1)}, u32[]{:S(2)}, u32[]{:S(2)}) async-start(bf16[128,8,256]{2,0,1:T(8,128)(2,1)} %bitcast.65), calls=%async_computation.4 | async-start | bytes 1048576 | tf_op jit(solution)/shard_map/all_to_all | solution.py:389
  224.0 4.2 %fusion.1 = bf16[1,512,2048]{2,1,0:T(8,128)(2,1)} fusion(bf16[384,512]{1,0:T(8,128)(2,1)} %copy-done.26, bf16[384,512]{1,0:T(8,128)(2,1)} %copy-done.29, bf16[384,512]{1,0:T(8,128)(2,1)} %get-tuple-element.76, bf16[384,512]{1,0:T(8,128)(2,1)} %get-tuple-element.77, bf16[384,512]{1,0:T(8,128)(2,1)} %copy-done.27), kind=kOutput, calls=%fused_computation.5 | convolution fusion | flops 812646400 | bytes 4063232 | tf_op jit(solution)/shard_map/dot_general | solution.py:22
  228.3 2.6 fusion
  231.0 2.7 fusion.2
  233.7 4.3 %shard_map.210 = (bf16[128,512]{1,0:T(8,128)(2,1)}, f32[128,512]{1,0:T(8,128)S(1)}, f32[128,1024]{1,0:T(8,128)S(1)}, f32[128,16]{1,0:T(8,128)S(1)}) custom-call(bf16[128,1024]{1,0:T(8,128)(2,1)S(1)} %copy-done.1, bf16[128,512]{1,0:T(8,128)(2,1)S(1)} %copy-done.7, bf16[128,512]{1,0:T(8,128)(2,1)S(1)} %copy-done.6, f32[128,16]{1,0:T(8,128)S(1)} %copy.49.steps_ref, ...), custom_call_target="tpu_custom_call" | custom-call | flops 201326592 | bytes 2260992 | tf_op jit(solution)/shard_map/pallas_call | solution.py:49
  238.8 13.7 %all-gather.14.cloned.1.call-done = bf16[1024,1024]{1,0:T(8,128)(2,1)} async-done(((bf16[128,1024]{1,0:T(8,128)(2,1)}), bf16[1024,1024]{1,0:T(8,128)(2,1)}) %all-gather.14.cloned.1.call-update) | async-done | bytes 2097168 | tf_op jit(solution)/shard_map/all_gather | solution.py:340
  252.5 3.5 %fusion.34 = f32[256,1024]{1,0:T(8,128)} fusion(bf16[1024,256]{1,0:T(8,128)(2,1)} %bitcast.21, bf16[1024,1024]{1,0:T(8,128)(2,1)} %all-gather.14.cloned.1.call-done), kind=kOutput, calls=%fused_computation.61 | convolution fusion | flops 536870912 | bytes 3670016 | tf_op jit(solution)/shard_map/dot_general | solution.py:22
  256.0 26.2 %all-gather.20.cloned.1.call-done = bf16[32,256,128]{2,1,0:T(8,128)(2,1)} async-done(((bf16[4,256,128]{2,1,0:T(8,128)(2,1)}), bf16[32,256,128]{2,1,0:T(8,128)(2,1)}) %all-gather.20.cloned.1.call-update) | async-done | bytes 2097168 | tf_op jit(solution)/shard_map/all_gather | solution.py:387
  284.8 2.6 shard_map.211
  (141 shorter events, 29.7 us)
Async XLA Ops:
  7.2 88.0 %copy-start = (bf16[1,512,2048]{2,1,0:T(8,128)(2,1)S(1)}, bf16[1,512,2048]{2,1,0:T(8,128)(2,1)}, u32[]{:S(2)}) copy-start(bf16[1,512,2048]{2,1,0:T(8,128)(2,1)} %param.25) | copy-start | bytes 6291460
  7.2 39.9 %copy-start.1 = (bf16[128,1024]{1,0:T(8,128)(2,1)S(1)}, bf16[128,1024]{1,0:T(8,128)(2,1)}, u32[]{:S(2)}) copy-start(bf16[128,1024]{1,0:T(8,128)(2,1)} %v_ref.5) | copy-start | bytes 786436
  7.2 53.7 %all-gather.10.cloned.1.call-start = ((), (), s32[]{:S(2)}) async-start(), calls=%async_computation.5 | async-start | bytes 1966080 | tf_op jit(solution)/shard_map/all_gather | solution.py:308
  11.1 35.5 %copy-start.47 = (f32[128,16]{0,1:T(8,128)S(1)}, f32[128,16]{0,1:T(8,128)}, u32[]{:S(2)}) copy-start(f32[128,16]{0,1:T(8,128)} %param.18) | copy-start | bytes 24580
  11.1 35.6 %copy-start.24 = (f32[16]{0:T(128)S(1)}, f32[16]{0:T(128)}, u32[]{:S(2)}) copy-start(f32[16]{0:T(128)} %param.19) | copy-start | bytes 196
  11.1 36.0 %copy-start.6 = (bf16[128,512]{1,0:T(8,128)(2,1)S(1)}, bf16[128,512]{1,0:T(8,128)(2,1)}, u32[]{:S(2)}) copy-start(bf16[128,512]{1,0:T(8,128)(2,1)} %c_ref.7) | copy-start | bytes 393220
  11.1 36.0 %copy-start.7 = (bf16[128,512]{1,0:T(8,128)(2,1)S(1)}, bf16[128,512]{1,0:T(8,128)(2,1)}, u32[]{:S(2)}) copy-start(bf16[128,512]{1,0:T(8,128)(2,1)} %b_ref.5) | copy-start | bytes 393220
  12.1 18.8 %copy-start.22 = (bf16[128,384]{1,0:T(8,128)(2,1)}, bf16[128,384]{1,0:T(8,128)(2,1)S(1)}, u32[]{:S(2)}) copy-start(bf16[128,384]{1,0:T(8,128)(2,1)S(1)} %get-tuple-element.29.sel_ref) | copy-start | bytes 294916
  30.9 62.7 %all-gather.12.cloned.1.call-start = ((), (), s32[]{:S(2)}) async-start(), calls=%async_computation.6 | async-start | bytes 1966080 | tf_op jit(solution)/shard_map/all_gather | solution.py:308
  46.6 78.4 %all-gather.18.cloned.1.call-start = ((), (), s32[]{:S(2)}) async-start(), calls=%async_computation.10 | async-start | bytes 2359296 | tf_op jit(solution)/shard_map/all_gather | solution.py:332
  50.4 108.6 %reduce-scatter.2.cloned.1.call-start = ((), (), s32[]{:S(2)}) async-start(), calls=%async_computation.7 | async-start | bytes 1966080 | tf_op jit(solution)/shard_map/reduce_scatter | solution.py:368
  63.3 33.0 %copy-start.27 = (bf16[384,512]{1,0:T(8,128)(2,1)}, bf16[384,512]{1,0:T(8,128)(2,1)S(1)}, u32[]{:S(2)}) copy-start(bf16[384,512]{1,0:T(8,128)(2,1)S(1)} %get-tuple-element.74) | copy-start | bytes 1179652
  63.3 33.0 %copy-start.29 = (bf16[384,512]{1,0:T(8,128)(2,1)}, bf16[384,512]{1,0:T(8,128)(2,1)S(1)}, u32[]{:S(2)}) copy-start(bf16[384,512]{1,0:T(8,128)(2,1)S(1)} %get-tuple-element.75) | copy-start | bytes 1179652
  103.8 21.2 %copy-start.8 = (bf16[128,1024]{1,0:T(8,128)(2,1)S(1)}, bf16[128,1024]{1,0:T(8,128)(2,1)}, u32[]{:S(2)}) copy-start(bf16[128,1024]{1,0:T(8,128)(2,1)} %gate_ref.3) | copy-start | bytes 786436
  103.9 107.8 %all-gather.16.cloned.1.call-start = ((), (), s32[]{:S(2)}) async-start(), calls=%async_computation.9 | async-start | bytes 4718592 | tf_op jit(solution)/shard_map/all_gather | solution.py:339
  103.9 79.0 %copy-start.5 = (bf16[128,2048]{1,0:T(8,128)(2,1)S(1)}, bf16[128,2048]{1,0:T(8,128)(2,1)}, u32[]{:S(2)}) copy-start(bf16[128,2048]{1,0:T(8,128)(2,1)} %g_ref.3) | copy-start | bytes 1572868
  104.5 148.1 %all-gather.14.cloned.1.call-start = ((), (), s32[]{:S(2)}) async-start(), calls=%async_computation.8 | async-start | bytes 2359296 | tf_op jit(solution)/shard_map/all_gather | solution.py:340
  130.8 151.4 %all-gather.20.cloned.1.call-start = ((), (), s32[]{:S(2)}) async-start(), calls=%async_computation.11 | async-start | bytes 2359296 | tf_op jit(solution)/shard_map/all_gather | solution.py:387
  194.6 20.1 %copy-start.12 = (f32[128,1024]{1,0:T(8,128)S(1)}, f32[128,1024]{1,0:T(8,128)}, u32[]{:S(2)}) copy-start(f32[128,1024]{1,0:T(8,128)} %copy-done.11) | copy-start | bytes 1572868
  194.6 23.0 %copy-start.46 = (f32[8,1,16]{2,1,0:T(1,128)S(1)}, f32[8,1,16]{2,1,0:T(1,128)}, u32[]{:S(2)}) copy-start(f32[8,1,16]{2,1,0:T(1,128)} %copy-done.45) | copy-start | bytes 1540
  219.6 32.9 %all-to-all-start.3 = ((bf16[128,8,256]{2,0,1:T(8,128)(2,1)}), bf16[128,8,256]{2,0,1:T(8,128)(2,1)}, u32[]{:S(2)}, u32[]{:S(2)}) async-start(bf16[128,8,256]{2,0,1:T(8,128)(2,1)} %bitcast.65), calls=%async_computation.4 | async-start | bytes 1048576 | tf_op jit(solution)/shard_map/all_to_all | solution.py:389
  224.0 4.3 %copy-start.28 = (bf16[384,512]{1,0:T(8,128)(2,1)S(1)}, bf16[384,512]{1,0:T(8,128)(2,1)}, u32[]{:S(2)}) copy-start(bf16[384,512]{1,0:T(8,128)(2,1)} %copy-done.27) | copy-start | bytes 1179652
  224.0 4.2 %copy-start.30 = (bf16[384,512]{1,0:T(8,128)(2,1)S(1)}, bf16[384,512]{1,0:T(8,128)(2,1)}, u32[]{:S(2)}) copy-start(bf16[384,512]{1,0:T(8,128)(2,1)} %copy-done.29) | copy-start | bytes 1179652
  224.0 4.2 %copy-start.32 = (bf16[384,512]{1,0:T(8,128)(2,1)S(1)}, bf16[384,512]{1,0:T(8,128)(2,1)}, u32[]{:S(2)}) copy-start(bf16[384,512]{1,0:T(8,128)(2,1)} %get-tuple-element.76) | copy-start | bytes 1179652
  (37 other events, 69.7 us)
Sparse Core Ops, SparseCore 0:
  31.0 29.8 all-gather.9
  62.7 30.8 all-gather.11
  95.8 29.1 all-gather.17
  128.4 30.5 reduce-scatter.1
  160.4 51.1 all-gather.15
  213.7 38.7 all-gather.13
  254.1 27.9 all-gather.19

commit v2 on v1

--- a/solution.py
+++ b/solution.py
@@ -8,6 +8,8 @@
 from jax.sharding import PartitionSpec as P
 
 NSTATE = 128
+TAIL = 16
+TERMS = 3
 CLAMP_LIMIT = 7.0
 SIGMOID_SCALE = 1.702
 HIGHEST = lax.Precision.HIGHEST
@@ -118,14 +120,25 @@
             att = (scores * mixing_of(log_ref, logt_ref, h)).astype(BF16)
             parts.append(mm(att, x[:, h * size : (h + 1) * size]))
         y_ref[:, g * wide : (g + 1) * wide] = jnp.concatenate(parts, axis=1)
-        state_ref[g] = mm(xe[:, g * wide : (g + 1) * wide], keys, TN).astype(BF16)
+        state_ref[g * wide : (g + 1) * wide, :] = mm(
+            xe[:, g * wide : (g + 1) * wide], keys, TN
+        ).astype(BF16)
+    at, lane = grid_of(heads, NSTATE)
+    rest = mm_exact(log_ref[length - 1 :, :], (at == lane).astype(F32))
+    row, _ = grid_of(TAIL, NSTATE)
+    tail = jnp.zeros((TAIL, NSTATE), F32)
+    for k in range(TERMS):
+        term = rest.astype(BF16).astype(F32)
+        tail = jnp.where(row == k, term, tail)
+        rest = rest - term
+    state_ref[groups * wide :, :] = tail.astype(BF16)
 
 
 def weighted_state(all_ref, weights_ref, g, r, per, size):
     h = g * per + r
     total = jnp.zeros((size, NSTATE), F32)
     for j in range(all_ref.shape[0]):
-        part = all_ref[j, g, r * size : (r + 1) * size, :].astype(F32)
+        part = all_ref[j, h * size : (h + 1) * size, :].astype(F32)
         total = total + weights_ref[j : j + 1, h : h + 1] * part
     return total
 
@@ -161,7 +174,7 @@
         mixer = grad * gate * sig
         mixer_ref[:, at] = mixer
         keys = c_ref[:, g * NSTATE : (g + 1) * NSTATE]
-        state_ref[g] = mm((mixer * decay[:, at]).astype(BF16), keys, TN).astype(BF16)
+        state_ref[at, :] = mm((mixer * decay[:, at]).astype(BF16), keys, TN).astype(BF16)
 
 
 def inner_kernel(
@@ -294,22 +307,6 @@
     state_shape = (groups, wide, NSTATE)
     pair_flops = 2 * tok_rows * tok_rows * inner
 
-    send_rows, send_grad, chosen = call(
-        functools.partial(dispatch_kernel, experts, cap, width),
-        [out((slots, width), BF16), out((slots, width), BF16), out((tok_rows, slots), BF16)],
-        6 * tok_rows * slots * width,
-        routes, route_weights, expert_inputs, stream_grad,
-    )
-
-    def to_experts(rows):
-        got = lax.all_to_all(
-            rows.reshape(experts, cap, width), "sp", split_axis=0, concat_axis=0, tiled=True
-        )
-        return lax.all_gather(got.reshape(slots, width), "tp", axis=0)
-
-    in_rows = side_by_side(to_experts(send_rows))
-    grad_rows = side_by_side(to_experts(send_grad))
-
     row, col = grid_of(tok_rows, tok_rows)
     rates = decay_rates.reshape(1, heads)
     drop = -step_sizes * rates
@@ -317,11 +314,34 @@
     log_decay_t = log_decay.T
     y_local, own_state = call(
         functools.partial(local_kernel, groups),
-        [out((tok_rows, inner), F32), out(state_shape, BF16)],
+        [out((tok_rows, inner), F32), out((inner + TAIL, NSTATE), BF16)],
         3 * pair_flops,
         mix_values, input_keys, output_keys, step_sizes, log_decay, log_decay_t,
     )
-    spans = lax.all_gather(log_decay[tok_rows - 1], "sp", axis=0)
+    all_states = lax.all_gather(own_state, "sp", axis=0)
+
+    send_rows, send_grad, chosen = call(
+        functools.partial(dispatch_kernel, experts, cap, width),
+        [out((slots, width), BF16), out((slots, width), BF16), out((tok_rows, slots), BF16)],
+        6 * tok_rows * slots * width,
+        routes, route_weights, expert_inputs, stream_grad,
+    )
+
+    def over_sp(rows):
+        return lax.all_to_all(
+            rows.reshape(experts, cap, width), "sp", split_axis=0, concat_axis=0, tiled=True
+        ).reshape(slots, width)
+
+    def over_tp(part):
+        copies = jnp.broadcast_to(part[None], (tp_devices,) + part.shape)
+        return lax.all_to_all(copies, "tp", split_axis=0, concat_axis=0, tiled=True)
+
+    got_rows = over_sp(send_rows)
+    got_grad, all_states = lax.optimization_barrier((over_sp(send_grad), all_states))
+    in_rows = side_by_side(over_tp(got_rows))
+    grad_rows = side_by_side(over_tp(got_grad))
+
+    spans = jnp.sum(all_states[:, inner : inner + TERMS, :heads].astype(F32), axis=1)
     here = lax.axis_index("sp")
     order = jnp.arange(sp_devices)
     one, two = order[:, None], order[None, :]
@@ -329,16 +349,12 @@
     forward = jnp.where(one < here, jnp.exp(forward), 0.0)
     backward = mm_exact(((two < one) & (two > here)).astype(F32), spans)
     backward = jnp.where(one > here, jnp.exp(backward), 0.0)
-    all_states = lax.all_gather(own_state, "sp", axis=0)
     mixer_out, gated_out, state_in = call(
         functools.partial(enter_kernel, groups),
         [out((tok_rows, inner), F32), out((tok_rows, inner), BF16), out(state_shape, BF16)],
         2 * pair_flops,
         all_states, forward, y_local, mix_gate, output_keys, log_decay,
     )
-    full_proj = lax.all_gather(out_proj, "sp", axis=0, tiled=True)
-    all_gated = lax.all_gather(gated_out, "sp", axis=0, tiled=True)
-
     gate_weight = gate_proj.reshape(-1, model_width)
     up_weight = up_proj.reshape(-1, model_width)
     down_weight = down_proj.reshape(-1, model_width)
@@ -365,7 +381,12 @@
     grad_gate_proj = mm(gate_grad, in_rows, TN).astype(BF16).reshape(gate_proj.shape)
     grad_up_proj = mm(up_grad, in_rows, TN).astype(BF16).reshape(up_proj.shape)
 
-    reduced = lax.psum_scatter(back, "tp", scatter_dimension=1, tiled=True)
+    full_proj = lax.all_gather(out_proj, "sp", axis=0, tiled=True)
+    back, full_proj, gated_out = lax.optimization_barrier((back, full_proj, gated_out))
+    all_gated = lax.all_gather(gated_out, "sp", axis=0, tiled=True)
+    shares = jnp.stack([back[:, c * width : (c + 1) * width] for c in range(tp_devices)])
+    shares = lax.all_to_all(shares, "tp", split_axis=0, concat_axis=0, tiled=True)
+    reduced = jnp.sum(shares.astype(F32), axis=0).astype(BF16)
     returned = lax.all_to_all(
         reduced.reshape(experts, cap, width), "sp", split_axis=0, concat_axis=0, tiled=True
     ).reshape(slots, width)
@@ -375,12 +396,13 @@
         2 * tok_rows * slots * width,
         chosen, returned, stream_grad,
     )[0]
+    stream_part, all_gated = lax.optimization_barrier((stream_part, all_gated))
     stream_total = lax.all_gather(stream_part, "tp", axis=1, tiled=True)
 
     gated_grad = mm(stream_total, full_proj)
     grad_gate, mixer_grad, own_grad = call(
         functools.partial(gate_kernel, groups),
-        [out((tok_rows, inner), BF16), out((tok_rows, inner), F32), out(state_shape, BF16)],
+        [out((tok_rows, inner), BF16), out((tok_rows, inner), F32), out((inner, NSTATE), BF16)],
         pair_flops,
         gated_grad, mixer_out, mix_gate, output_keys, log_decay,
     )

time: 296 us -> 235 us (0.79)
  waiting for transfers between devices: 134 us -> 46.3 us
  blocking collectives: 80.9 us -> 92.3 us
  starting transfers between devices: 4.6 us -> 13.2 us
  matrix products: 23.2 us -> 26.8 us
    all_gather x2 -> x0, waiting for transfers between devices: 40.8 us -> none  [to_experts(): return lax.all_gather(got.reshape(slots, width), 'tp', axis=0)]
    all_to_all x2 -> x3, blocking collectives: 34.4 us -> 67 us  [the longest x2 44.5 us: over_sp(): lax.all_to_all(rows.reshape(experts, cap, width), 'sp', split_axis=0, con...]
    all_to_all x0 -> x2, waiting for transfers between devices: none -> 30.5 us  [over_tp(): return lax.all_to_all(copies, 'tp', split_axis=0, concat_axis=0, tiled=True)]
    reduce_scatter x1 -> x0, waiting for transfers between devices: 28.1 us -> none  [body(): reduced = lax.psum_scatter(back, 'tp', scatter_dimension=1, tiled=True)]
    all_gather x1, waiting for transfers between devices: 26.2 us -> 1.29 us  [body(): all_grads = lax.all_gather(own_grad, 'sp', axis=0)]
    all_gather x1, waiting for transfers between devices: 17 us -> 0.01 us  [body(): full_proj = lax.all_gather(out_proj, 'sp', axis=0, tiled=True)]
    all_to_all x1, waiting for transfers between devices: 0.01 us -> 13.7 us  [body(): lax.all_to_all(stream_total, 'sp', split_axis=1, concat_axis=0, tiled=True)]
    all_gather x1, waiting for transfers between devices: 13.7 us -> 0.02 us  [body(): all_gated = lax.all_gather(gated_out, 'sp', axis=0, tiled=True)]
  transfers between devices with their start and end apart: 8 -> 7, of which waited for: 7 -> 4; matrix products, arithmetic and copies ran while one was open for 10% -> 15% of each run, Pallas kernels for 3% -> 3%
where the time goes in v2:
time: 235 us; the launch traced here: 234 us
  blocking collectives  92.3 us (39%)
  waiting for transfers between devices  46.3 us (20%)
  matrix products  26.8 us (11%)
  local copies, waits for them, and re-layouts  24.9 us (11%)
  between operations  14.3 us (6%)
  Pallas kernels  13.6 us (6%)
  starting transfers between devices  13.2 us (6%)
  other arithmetic  2.8 us (1%)
    all_to_all x2, blocking collectives, over_sp(): lax.all_to_all(rows.reshape(experts, cap, width), 'sp', split_axis=0, con...  44.5 us
    all_to_all x2, waiting for transfers between devices, over_tp(): return lax.all_to_all(copies, 'tp', split_axis=0, concat_axis=0, tiled=True)  30.5 us
    dot_general x10, matrix products, mm(): return lax.dot_general(a, b, dims, preferred_element_type=F32)  25.7 us
    all_to_all x1, blocking collectives, body(): lax.all_to_all(shares, 'tp', split_axis=0, concat_axis=0, tiled=True)  22.5 us
    unnamed x104, local copies, waits for them, and re-layouts  16.8 us
    all_to_all x1, blocking collectives, body(): lax.all_to_all(reduced.reshape(experts, cap, width), 'sp', split_axis=0,...  15.9 us
    all_to_all x1, waiting for transfers between devices, body(): lax.all_to_all(stream_total, 'sp', split_axis=1, concat_axis=0, tiled=True)  13.7 us
    pallas_call x7, Pallas kernels, call(): pl.pallas_call(kernel, out_shape=outs, in_specs=[pl.BlockSpec(memory_spac...  13.6 us
  transfers between devices with their start and end apart: 7, of which 4 were waited for; matrix products, arithmetic and copies ran while one was open for 15% of the time, Pallas kernels for 3%

profile of v2, /device:TPU:0, one launch (start us, length us, event | category | flops | bytes accessed | tf_op | source)
XLA Modules:
  0.0 234.2 jit_solution(17987766359438065075)
XLA Ops:
  12.0 2.5 %shard_map.206 = (f32[128,1024]{1,0:T(8,128)S(1)}, bf16[1040,128]{1,0:T(8,128)(2,1)}) custom-call(bf16[128,1024]{1,0:T(8,128)(2,1)S(1)} %copy-done.1, bf16[128,512]{1,0:T(8,128)(2,1)S(1)} %copy-done.9, bf16[128,512]{1,0:T(8,128)(2,1)S(1)} %copy-done.7, f32[128,16]{1,0:T(8,128)S(1)} %copy.36.steps_ref, f32[128,16]{1,0:T(8,128)S(1)} %copy.37.log_ref, ...), custom_call_target="tpu_custom_call" | custom-call | flops 100663296 | bytes 1339392 | tf_op jit(solution)/shard_map/pallas_call | solution.py:51
  20.7 29.6 %all_to_all.49 = bf16[8,48,512]{2,1,0:T(8,128)(2,1)S(1)} all-to-all(bf16[8,48,512]{2,1,0:T(8,128)(2,1)S(1)} %bitcast.77), channel_id=1, replica_groups=mesh['sp'=8,'tp'=4] {'sp'}, dimensions={0} | all-to-all | bytes 786432 | tf_op jit(solution)/shard_map/all_to_all | solution.py:331
  50.3 14.9 %all_to_all.50 = bf16[8,48,512]{2,1,0:T(8,128)(2,1)S(1)} all-to-all(bf16[8,48,512]{2,1,0:T(8,128)(2,1)S(1)} %bitcast.76), channel_id=1, replica_groups=mesh['sp'=8,'tp'=4] {'sp'}, dimensions={0} | all-to-all | bytes 786432 | tf_op jit(solution)/shard_map/all_to_all | solution.py:331
  66.5 4.3 %all-to-all-start.1 = ((bf16[4,384,512]{2,1,0:T(8,128)(2,1)}), bf16[4,384,512]{2,1,0:T(8,128)(2,1)}, u32[]{:S(2)}, u32[]{:S(2)}) async-start(bf16[4,384,512]{2,1,0:T(8,128)(2,1)} %broadcast_in_dim.39), calls=%async_computation.1 | async-start | bytes 3145728 | tf_op jit(solution)/shard_map/all_to_all | solution.py:337
  70.9 19.4 %all-to-all-done.1 = bf16[4,384,512]{2,1,0:T(8,128)(2,1)} async-done(((bf16[4,384,512]{2,1,0:T(8,128)(2,1)}), bf16[4,384,512]{2,1,0:T(8,128)(2,1)}, u32[]{:S(2)}, u32[]{:S(2)}) %all-to-all-start.1) | async-done | bytes 1572896 | tf_op jit(solution)/shard_map/all_to_all | solution.py:337
  91.5 4.4 %all-to-all-start.3 = ((bf16[4,384,512]{2,1,0:T(8,128)(2,1)}), bf16[4,384,512]{2,1,0:T(8,128)(2,1)}, u32[]{:S(2)}, u32[]{:S(2)}) async-start(bf16[4,384,512]{2,1,0:T(8,128)(2,1)} %broadcast_in_dim.40), calls=%async_computation.3 | async-start | bytes 3145728 | tf_op jit(solution)/shard_map/all_to_all | solution.py:337
  97.5 1.9 fusion.10
  99.9 1.9 fusion.4
  103.6 11.1 %all-to-all-done.3 = bf16[4,384,512]{2,1,0:T(8,128)(2,1)} async-done(((bf16[4,384,512]{2,1,0:T(8,128)(2,1)}), bf16[4,384,512]{2,1,0:T(8,128)(2,1)}, u32[]{:S(2)}, u32[]{:S(2)}) %all-to-all-start.3) | async-done | bytes 1572896 | tf_op jit(solution)/shard_map/all_to_all | solution.py:337
  116.9 2.6 %select_convert_fusion = (bf16[384,512]{1,0:T(8,128)(2,1)S(1)}, bf16[384,512]{1,0:T(8,128)(2,1)S(1)}) fusion(f32[384,512]{1,0:T(8,128)} %fusion.4, f32[384,512]{1,0:T(8,128)S(1)} %copy-done.47, bf16[1,512,2048]{2,1,0:T(8,128)(2,1)S(1)} %copy-done.46, bf16[384,512]{1,0:T(8,128)(2,1)S(1)} %get-tuple-element.88, bf16[384,512]{1,0:T(8,128)(2,1)S(1)} %get-tuple-element.89, ...), kind=kOutput, calls=%fused_computation.24 | convolution fusion | flops 815923200 | bytes 6029312 | tf_op jit(solution)/shard_map/dot_general | solution.py:24
  121.5 2.1 add_convert_fusion
  125.4 22.5 %all_to_all.51 = bf16[4,384,512]{2,1,0:T(8,128)(2,1)} all-to-all(bf16[4,384,512]{2,1,0:T(8,128)(2,1)S(1)} %pad_maximum_fusion.2), channel_id=1, replica_groups=mesh['sp'=8,'tp'=4] {'tp'}, dimensions={0} | all-to-all | bytes 3145728 | tf_op jit(solution)/shard_map/all_to_all | solution.py:388
  147.8 2.6 %reduce_sum.22 = bf16[384,512]{1,0:T(8,128)(2,1)} reduce(bf16[4,384,512]{2,1,0:T(8,128)(2,1)} %all_to_all.51, bf16[]{:T(256)} %constant.18.clone.1), dimensions={0}, to_apply=%region_1.2 | reduce | flops 589824 | bytes 1966082 | tf_op jit(solution)/shard_map/reduce_sum | solution.py:389
  150.4 15.9 %all_to_all.52 = bf16[8,48,512]{2,1,0:T(8,128)(2,1)S(1)} all-to-all(bf16[8,48,512]{2,1,0:T(8,128)(2,1)} %bitcast.83), channel_id=1, replica_groups=mesh['sp'=8,'tp'=4] {'sp'}, dimensions={0} | all-to-all | bytes 786432 | tf_op jit(solution)/shard_map/all_to_all | solution.py:390
  167.4 9.4 %all_gather.25 = bf16[128,2048]{1,0:T(8,128)(2,1)S(1)} all-gather(bf16[128,512]{1,0:T(8,128)(2,1)S(1)} %shard_map.208), channel_id=1, replica_groups=mesh['sp'=8,'tp'=4] {'tp'}, dimensions={1}, use_global_device_ids=true | all-gather | bytes 655360 | tf_op jit(solution)/shard_map/all_gather | solution.py:400
  176.9 3.0 %fusion.35.grad_ref = f32[128,1024]{1,0:T(8,128)S(1)} fusion(bf16[128,2048]{1,0:T(8,128)(2,1)S(1)} %all_gather.25, bf16[2048,1024]{1,0:T(8,128)(2,1)} %all-gather.7.cloned.1.call-done), kind=kOutput, calls=%fused_computation.67 | convolution fusion | flops 536870912 | bytes 5242880 | tf_op jit(solution)/shard_map/dot_general | solution.py:24
  183.8 4.3 %all-to-all-start.6 = ((bf16[128,8,256]{2,0,1:T(8,128)(2,1)}), bf16[128,8,256]{2,0,1:T(8,128)(2,1)}, u32[]{:S(2)}, u32[]{:S(2)}) async-start(bf16[128,8,256]{2,0,1:T(8,128)(2,1)} %bitcast.82), calls=%async_computation.6 | async-start | bytes 1048576 | tf_op jit(solution)/shard_map/all_to_all | solution.py:411
  188.2 4.4 %fusion.1 = bf16[1,512,2048]{2,1,0:T(8,128)(2,1)} fusion(bf16[384,512]{1,0:T(8,128)(2,1)} %copy-done.27, bf16[384,512]{1,0:T(8,128)(2,1)} %copy-done.30, bf16[384,512]{1,0:T(8,128)(2,1)} %copy-done.32, bf16[384,512]{1,0:T(8,128)(2,1)} %copy-done.34, bf16[384,512]{1,0:T(8,128)(2,1)} %copy-done.28), kind=kOutput, calls=%fused_computation.5 | convolution fusion | flops 812646400 | bytes 4063232 | tf_op jit(solution)/shard_map/dot_general | solution.py:24
  192.6 2.6 %fusion = bf16[1,512,2048]{2,1,0:T(8,128)(2,1)} fusion(bf16[384,512]{1,0:T(8,128)(2,1)S(1)} %copy-done.45, bf16[384,512]{1,0:T(8,128)(2,1)S(1)} %copy-done.31, bf16[384,512]{1,0:T(8,128)(2,1)S(1)} %copy-done.33, bf16[384,512]{1,0:T(8,128)(2,1)S(1)} %copy-done.35, bf16[384,512]{1,0:T(8,128)(2,1)S(1)} %copy-done.29), kind=kOutput, calls=%fused_computation.4 | convolution fusion | flops 812646400 | bytes 4063232 | tf_op jit(solution)/shard_map/dot_general | solution.py:24
  195.3 2.7 %fusion.2 = bf16[1,512,2048]{2,1,0:T(8,128)(2,1)} fusion(f32[384,512]{1,0:T(8,128)S(1)} %copy-done.48, f32[384,512]{1,0:T(8,128)S(1)} %copy-done.49, bf16[384,512]{1,0:T(8,128)(2,1)S(1)} %copy-done.39, bf16[384,512]{1,0:T(8,128)(2,1)S(1)} %copy-done.41, bf16[384,512]{1,0:T(8,128)(2,1)S(1)} %copy-done.43, bf16[384,512]{1,0:T(8,128)(2,1)S(1)} %copy-done.37), kind=kOutput, calls=%fused_computation.6 | convolution fusion | flops 814612480 | bytes 5242880 | tf_op jit(solution)/shard_map/dot_general | solution.py:24
  198.0 4.3 %shard_map.210 = (bf16[128,512]{1,0:T(8,128)(2,1)}, f32[128,512]{1,0:T(8,128)S(1)}, f32[128,1024]{1,0:T(8,128)S(1)}, f32[128,16]{1,0:T(8,128)S(1)}) custom-call(bf16[128,1024]{1,0:T(8,128)(2,1)S(1)} %copy-done.2, bf16[128,512]{1,0:T(8,128)(2,1)S(1)} %copy-done.10, bf16[128,512]{1,0:T(8,128)(2,1)S(1)} %copy-done.8, f32[128,16]{1,0:T(8,128)S(1)} %copy.36.steps_ref, ...), custom_call_target="tpu_custom_call" | custom-call | flops 201326592 | bytes 2260992 | tf_op jit(solution)/shard_map/pallas_call | solution.py:51
  203.2 13.7 %all-to-all-done.6 = bf16[128,8,256]{2,0,1:T(8,128)(2,1)} async-done(((bf16[128,8,256]{2,0,1:T(8,128)(2,1)}), bf16[128,8,256]{2,0,1:T(8,128)(2,1)}, u32[]{:S(2)}, u32[]{:S(2)}) %all-to-all-start.6) | async-done | bytes 524320 | tf_op jit(solution)/shard_map/all_to_all | solution.py:411
  216.9 3.5 %fusion.34 = f32[256,1024]{1,0:T(8,128)} fusion(bf16[1024,256]{1,0:T(8,128)(2,1)} %bitcast.27, bf16[1024,1024]{1,0:T(8,128)(2,1)} %all-gather.9.cloned.1.call-done), kind=kOutput, calls=%fused_computation.66 | convolution fusion | flops 536870912 | bytes 3670016 | tf_op jit(solution)/shard_map/dot_general | solution.py:24
  224.3 2.6 %shard_map.211 = (bf16[128,1024]{1,0:T(8,128)(2,1)}, bf16[128,512]{1,0:T(8,128)(2,1)}, f32[128,16]{1,0:T(8,128)S(1)}) custom-call(bf16[8,1024,128]{2,1,0:T(8,128)(2,1)S(1)} %bitcast.74, f32[8,16]{1,0:T(8,128)S(1)} %fusion.13.weights_ref, bf16[4,256,128]{2,1,0:T(8,128)(2,1)S(1)} %get-tuple-element.49.state_ref, bf16[128,1024]{1,0:T(8,128)(2,1)S(1)} %copy-done.2, ...), custom_call_target="tpu_custom_call" | custom-call | flops 100663296 | bytes 3965504 | tf_op jit(solution)/shard_map/pallas_call | solution.py:51
  (135 shorter events, 33.6 us)
Async XLA Ops:
  7.2 90.3 %copy-start = (bf16[1,512,2048]{2,1,0:T(8,128)(2,1)S(1)}, bf16[1,512,2048]{2,1,0:T(8,128)(2,1)}, u32[]{:S(2)}) copy-start(bf16[1,512,2048]{2,1,0:T(8,128)(2,1)} %param.25) | copy-start | bytes 6291460
  7.2 63.7 %all-gather.11.cloned.1.call-start = ((), (), s32[]{:S(2)}) async-start(), calls=%async_computation.9 | async-start | bytes 2396160 | tf_op jit(solution)/shard_map/all_gather | solution.py:321
  15.3 108.3 %all-gather.7.cloned.1.call-start = ((), (), s32[]{:S(2)}) async-start(), calls=%async_computation.7 | async-start | bytes 4718592 | tf_op jit(solution)/shard_map/all_gather | solution.py:384
  20.7 44.5 %copy-start.22 = (bf16[128,384]{1,0:T(8,128)(2,1)}, bf16[128,384]{1,0:T(8,128)(2,1)S(1)}, u32[]{:S(2)}) copy-start(bf16[128,384]{1,0:T(8,128)(2,1)S(1)} %get-tuple-element.38.sel_ref) | copy-start | bytes 294916
  66.5 23.8 %all-to-all-start.1 = ((bf16[4,384,512]{2,1,0:T(8,128)(2,1)}), bf16[4,384,512]{2,1,0:T(8,128)(2,1)}, u32[]{:S(2)}, u32[]{:S(2)}) async-start(bf16[4,384,512]{2,1,0:T(8,128)(2,1)} %broadcast_in_dim.39), calls=%async_computation.1 | async-start | bytes 3145728 | tf_op jit(solution)/shard_map/all_to_all | solution.py:337
  91.5 23.2 %all-to-all-start.3 = ((bf16[4,384,512]{2,1,0:T(8,128)(2,1)}), bf16[4,384,512]{2,1,0:T(8,128)(2,1)}, u32[]{:S(2)}, u32[]{:S(2)}) async-start(bf16[4,384,512]{2,1,0:T(8,128)(2,1)} %broadcast_in_dim.40), calls=%async_computation.3 | async-start | bytes 3145728 | tf_op jit(solution)/shard_map/all_to_all | solution.py:337
  95.9 71.5 %all-gather.9.cloned.1.call-start = ((), (), s32[]{:S(2)}) async-start(), calls=%async_computation.8 | async-start | bytes 2359296 | tf_op jit(solution)/shard_map/all_gather | solution.py:386
  103.6 16.0 %copy-start.12 = (f32[128,1024]{1,0:T(8,128)}, f32[128,1024]{1,0:T(8,128)S(1)}, u32[]{:S(2)}) copy-start(f32[128,1024]{1,0:T(8,128)S(1)} %get-tuple-element.47.out_ref) | copy-start | bytes 1572868
  116.3 3.2 %copy-start.36 = (bf16[384,512]{1,0:T(8,128)(2,1)}, bf16[384,512]{1,0:T(8,128)(2,1)S(1)}, u32[]{:S(2)}) copy-start(bf16[384,512]{1,0:T(8,128)(2,1)S(1)} %get-tuple-element.87) | copy-start | bytes 1179652
  116.3 3.2 %copy-start.38 = (bf16[384,512]{1,0:T(8,128)(2,1)}, bf16[384,512]{1,0:T(8,128)(2,1)S(1)}, u32[]{:S(2)}) copy-start(bf16[384,512]{1,0:T(8,128)(2,1)S(1)} %get-tuple-element.88) | copy-start | bytes 1179652
  116.3 3.2 %copy-start.40 = (bf16[384,512]{1,0:T(8,128)(2,1)}, bf16[384,512]{1,0:T(8,128)(2,1)S(1)}, u32[]{:S(2)}) copy-start(bf16[384,512]{1,0:T(8,128)(2,1)S(1)} %get-tuple-element.89) | copy-start | bytes 1179652
  116.4 3.2 %copy-start.42 = (bf16[384,512]{1,0:T(8,128)(2,1)}, bf16[384,512]{1,0:T(8,128)(2,1)S(1)}, u32[]{:S(2)}) copy-start(bf16[384,512]{1,0:T(8,128)(2,1)S(1)} %get-tuple-element.90) | copy-start | bytes 1179652
  123.6 98.1 %all-gather.13.cloned.1.call-start = ((), (), s32[]{:S(2)}) async-start(), calls=%async_computation.10 | async-start | bytes 2359296 | tf_op jit(solution)/shard_map/all_gather | solution.py:409
  147.8 18.4 %copy-start.6 = (bf16[128,2048]{1,0:T(8,128)(2,1)S(1)}, bf16[128,2048]{1,0:T(8,128)(2,1)}, u32[]{:S(2)}) copy-start(bf16[128,2048]{1,0:T(8,128)(2,1)} %g_ref.3) | copy-start | bytes 1572868
  176.8 3.0 %copy-start.13 = (f32[128,1024]{1,0:T(8,128)S(1)}, f32[128,1024]{1,0:T(8,128)}, u32[]{:S(2)}) copy-start(f32[128,1024]{1,0:T(8,128)} %copy-done.12) | copy-start | bytes 1572868
  183.8 33.1 %all-to-all-start.6 = ((bf16[128,8,256]{2,0,1:T(8,128)(2,1)}), bf16[128,8,256]{2,0,1:T(8,128)(2,1)}, u32[]{:S(2)}, u32[]{:S(2)}) async-start(bf16[128,8,256]{2,0,1:T(8,128)(2,1)} %bitcast.82), calls=%async_computation.6 | async-start | bytes 1048576 | tf_op jit(solution)/shard_map/all_to_all | solution.py:411
  188.1 4.4 %copy-start.29 = (bf16[384,512]{1,0:T(8,128)(2,1)S(1)}, bf16[384,512]{1,0:T(8,128)(2,1)}, u32[]{:S(2)}) copy-start(bf16[384,512]{1,0:T(8,128)(2,1)} %copy-done.28) | copy-start | bytes 1179652
  188.1 4.4 %copy-start.31 = (bf16[384,512]{1,0:T(8,128)(2,1)S(1)}, bf16[384,512]{1,0:T(8,128)(2,1)}, u32[]{:S(2)}) copy-start(bf16[384,512]{1,0:T(8,128)(2,1)} %copy-done.30) | copy-start | bytes 1179652
  188.1 4.4 %copy-start.33 = (bf16[384,512]{1,0:T(8,128)(2,1)S(1)}, bf16[384,512]{1,0:T(8,128)(2,1)}, u32[]{:S(2)}) copy-start(bf16[384,512]{1,0:T(8,128)(2,1)} %copy-done.32) | copy-start | bytes 1179652
  188.1 4.4 %copy-start.35 = (bf16[384,512]{1,0:T(8,128)(2,1)S(1)}, bf16[384,512]{1,0:T(8,128)(2,1)}, u32[]{:S(2)}) copy-start(bf16[384,512]{1,0:T(8,128)(2,1)} %copy-done.34) | copy-start | bytes 1179652
  188.2 4.4 %copy-start.45 = (bf16[384,512]{1,0:T(8,128)(2,1)S(1)}, bf16[384,512]{1,0:T(8,128)(2,1)}, u32[]{:S(2)}) copy-start(bf16[384,512]{1,0:T(8,128)(2,1)} %copy-done.44) | copy-start | bytes 1179652
  195.3 2.8 %copy-start.2 = (bf16[128,1024]{1,0:T(8,128)(2,1)S(1)}, bf16[128,1024]{1,0:T(8,128)(2,1)}, u32[]{:S(2)}) copy-start(bf16[128,1024]{1,0:T(8,128)(2,1)} %v_ref.5) | copy-start | bytes 786436
  195.3 2.8 %copy-start.10 = (bf16[128,512]{1,0:T(8,128)(2,1)S(1)}, bf16[128,512]{1,0:T(8,128)(2,1)}, u32[]{:S(2)}) copy-start(bf16[128,512]{1,0:T(8,128)(2,1)} %b_ref.5) | copy-start | bytes 393220
  203.2 18.5 %copy-start.24 = (f32[16]{0:T(128)S(1)}, f32[16]{0:T(128)}, u32[]{:S(2)}) copy-start(f32[16]{0:T(128)} %param.19) | copy-start | bytes 196
  (33 other events, 56.9 us)
Sparse Core Ops, SparseCore 0:
  15.4 41.0 all-gather.10
  58.0 45.4 all-gather.6
  123.8 27.6 all-gather.8
  182.9 38.7 all-gather.12
